TPU v7x, 32 devices: a whole 2x2x4 slice. The times are simulated.
32 devices in a mesh: ep: 8 (over z, x), tp: 4 (over y, core).
Axes of the slice: x: 2, y: 2, z: 4, core: 2. Of those that a mesh axis runs over, the one named last changes fastest.
Arguments:
- queries: bfloat16 [1024, 512], P('ep'), may hold values from -6 to 6
- key_vectors: bfloat16 [1024, 512], P('ep'), may hold values from -6 to 6
- values: bfloat16 [1024, 1024], P('ep', 'tp'), may hold values from -6 to 6
- out_gate: bfloat16 [1024, 1024], P('ep', 'tp'), may hold values from -6 to 6
- input_gate: float32 [1024, 2], P('ep'), may hold values from -8 to 130
- forget_gate: float32 [1024, 2], P('ep'), may hold values from -2 to 16
- mix_weight: bfloat16 [1024, 2048], P('tp'), may hold values from -0.1875 to 0.1875
- expert_input: bfloat16 [2048, 2048], P('ep'), may hold values from -6 to 6
- norm_gain: float32 [2048], replicated, may hold values from 0.1 to 1.9
- route_ids: int32 [2048, 4], P('ep'), may hold values from 0 to 7, all different within a row; in each aligned block of 256 rows (0 to 255, 256 to 511, ...) at most 256 rows name the same one
- route_weights: float32 [2048, 4], P('ep'), may hold values from 0.2 to 1.2
- expert_gate: bfloat16 [32, 2048, 256], P(('ep', 'tp')), may hold values from -0.125 to 0.125
- expert_up: bfloat16 [32, 2048, 256], P(('ep', 'tp')), may hold values from -0.125 to 0.125
- expert_down: bfloat16 [32, 256, 2048], P(('ep', 'tp')), may hold values from -0.1875 to 0.1875
- shared_gate: bfloat16 [2048, 512], P(None, 'tp'), may hold values from -0.125 to 0.125
- shared_up: bfloat16 [2048, 512], P(None, 'tp'), may hold values from -0.125 to 0.125
- shared_down: bfloat16 [512, 2048], P('tp'), may hold values from -0.25 to 0.25
Outputs:
- mixer_out: bfloat16 [1024, 2048], P('ep')
- expert_out: bfloat16 [2048, 2048], P('ep')
Inputs may be any that keep to these rules, and one draw needn't show every extreme that they name: `route_ids`: each row names 4 different experts. In each aligned block of 256 rows (the rows of one index of ep) no expert is named by more than 256 rows, and in some block one expert is named by exactly 256 rows.
All inputs are finite; a program needn't handle non-finite values.
Results may differ from a plain program's by a relative error of at most 0.01575.
Values may be sent and summed in bfloat16 or wider, within the bound.
A program may use at most 64 MiB of HBM per device.

v0:
```python
import jax
import jax.numpy as jnp
from jax import lax
from jax.sharding import PartitionSpec as P

D = 2048
MEMORY_HEADS = 2
KEY_DIM = 256
BLOCK = 128
FF = 1024


epsilon = 1e-06
lowest = -1e30
den_floor = 4.0


def prefix_2(value, axis, join, neutral):
    count, mine = (lax.axis_size(axis), lax.axis_index(axis))
    pieces = jax.tree.map(lambda part: lax.all_gather(part, axis), value)
    subtotal = jax.tree.map(
        lambda part, zero: jnp.full_like(part, 0) + jnp.asarray(zero, part.dtype), value, neutral
    )

    def turn(position, subtotal):
        longer = join(subtotal, jax.tree.map(lambda part: part[position], pieces))
        return jax.tree.map(lambda new, old: jnp.where(position < mine, new, old), longer, subtotal)

    return lax.fori_loop(0, count - 1, turn, subtotal)


def combine_segments(earlier, later):
    first_decay, first_memory, first_normalizer, first_running = earlier
    second_decay, second_memory, second_normalizer, second_running = later
    running = jnp.maximum(second_decay + first_running, second_running)
    lead_scale = jnp.exp(second_decay + first_running - running)
    tail_scale = jnp.exp(second_running - running)
    return (
        first_decay + second_decay,
        lead_scale * first_memory + tail_scale * second_memory,
        lead_scale * first_normalizer + tail_scale * second_normalizer,
        running,
    )


def mixer_half(queries, key_vectors, values, out_gate, input_gate, forget_gate, mix_weight):
    tp_count = lax.axis_size("tp")
    tp_rank = lax.axis_index("tp")
    length = queries.shape[0]
    blocks = length // BLOCK
    channels = values.shape[1]
    factor = KEY_DIM ** (-0.5)
    head_index = tp_rank // (tp_count // MEMORY_HEADS)
    offset = head_index * KEY_DIM
    query_head = lax.dynamic_slice_in_dim(queries, offset, KEY_DIM, 1).reshape(
        blocks, BLOCK, KEY_DIM
    )
    key_head = lax.dynamic_slice_in_dim(key_vectors, offset, KEY_DIM, 1).reshape(
        blocks, BLOCK, KEY_DIM
    )
    value_blocks = values.reshape(blocks, BLOCK, channels)
    select = jnp.arange(MEMORY_HEADS, dtype=jnp.int32)[None, :] == head_index
    input_head = jnp.sum(jnp.where(select, input_gate, 0.0), axis=1).reshape(blocks, BLOCK)
    forget_head = jax.nn.log_sigmoid(jnp.sum(jnp.where(select, forget_gate, 0.0), axis=1)).reshape(
        blocks, BLOCK
    )
    cumulative = jnp.cumsum(forget_head, axis=1)
    block_total = cumulative[:, -1]
    log_retention = block_total[:, None] - cumulative + input_head
    block_running = jnp.max(log_retention, axis=1)
    weighted_keys = (
        key_head.astype(jnp.float32) * jnp.exp(log_retention - block_running[:, None])[:, :, None]
    )
    block_memory = jnp.einsum(
        "bsd,bsv->bdv",
        weighted_keys,
        value_blocks.astype(jnp.float32),
        precision=lax.Precision.HIGHEST,
    )
    block_normalizer = jnp.sum(weighted_keys, axis=1)
    segments = (block_total, block_memory, block_normalizer, block_running)
    neutral = (
        jnp.zeros((), jnp.float32),
        jnp.zeros((KEY_DIM, channels), jnp.float32),
        jnp.zeros((KEY_DIM,), jnp.float32),
        jnp.full((), lowest, jnp.float32),
    )

    def fold_block(carry_in, segment):
        return (combine_segments(carry_in, segment), None)

    summary, _ = lax.scan(fold_block, neutral, segments)
    prefix = prefix_2(summary, "ep", combine_segments, neutral)
    start_state = (
        jnp.zeros((), jnp.float32),
        jnp.zeros((KEY_DIM, channels), jnp.float32),
        jnp.zeros((KEY_DIM,), jnp.float32),
        jnp.zeros((), jnp.float32),
    )
    entering = combine_segments(start_state, prefix)
    causal = jnp.tril(jnp.ones((BLOCK, BLOCK), dtype=bool))

    def block_pass(carry_in, inputs):
        query_block, key_block, value_block, input_block, cumulative_block, segment = inputs
        _, memory, normalizer, running = carry_in
        carried = cumulative_block + running
        log_weight = cumulative_block[:, None] - cumulative_block[None, :] + input_block[None, :]
        log_weight = jnp.where(causal, log_weight, -jnp.inf)
        stabilizer = jnp.maximum(carried, jnp.max(log_weight, axis=1))
        within = jnp.exp(log_weight - stabilizer[:, None])
        across = jnp.exp(carried - stabilizer)
        scores = (
            jnp.einsum("td,sd->ts", query_block, key_block, preferred_element_type=jnp.float32)
            * factor
        )
        weights = scores * within
        scaled = query_block.astype(jnp.float32) * factor
        numerator = across[:, None] * jnp.dot(scaled, memory, precision=lax.Precision.HIGHEST)
        numerator = numerator + jnp.dot(
            weights.astype(jnp.bfloat16), value_block, preferred_element_type=jnp.float32
        )
        denominator = across * jnp.dot(scaled, normalizer, precision=lax.Precision.HIGHEST)
        denominator = denominator + jnp.sum(weights, axis=1)
        hidden = numerator / jnp.maximum(jnp.abs(denominator), den_floor)[:, None]
        return (combine_segments(carry_in, segment), hidden)

    _, hidden = lax.scan(
        block_pass, entering, (query_head, key_head, value_blocks, input_head, cumulative, segments)
    )
    gated_rows = (
        hidden.reshape(length, channels) * jax.nn.sigmoid(out_gate.astype(jnp.float32))
    ).astype(jnp.bfloat16)
    return jnp.dot(gated_rows, mix_weight, preferred_element_type=jnp.float32)


def expert_half(
    expert_input,
    norm_gain,
    route_ids,
    route_weights,
    expert_gate,
    expert_up,
    expert_down,
    shared_gate,
    shared_up,
    shared_down,
):
    ep_count = lax.axis_size("ep")
    tp_count = lax.axis_size("tp")
    tp_rank = lax.axis_index("tp")
    tokens = expert_input.shape[0]
    top_count = route_ids.shape[1]
    slice_units = expert_gate.shape[2]
    group_size = FF // slice_units
    per_ep = tp_count // group_size
    team_index = tp_rank // group_size
    expert_count = ep_count * per_ep
    capacity = 2 * tokens * top_count // expert_count
    rows_wide = expert_input.astype(jnp.float32)
    normed = (
        rows_wide
        * lax.rsqrt(jnp.mean(rows_wide * rows_wide, axis=-1, keepdims=True) + epsilon)
        * norm_gain
    ).astype(jnp.bfloat16)
    chosen = route_ids.reshape(-1)
    onehot = (chosen[:, None] == jnp.arange(expert_count, dtype=jnp.int32)[None, :]).astype(
        jnp.int32
    )
    slot_rank = jnp.sum((jnp.cumsum(onehot, axis=0) - onehot) * onehot, axis=1)
    in_team = chosen % per_ep == team_index
    target = jnp.where(in_team, chosen // per_ep * capacity + slot_rank, ep_count * capacity)
    token_of = jnp.arange(chosen.shape[0], dtype=jnp.int32) // top_count
    slot_token = jnp.zeros((ep_count * capacity,), jnp.int32).at[target].set(token_of, mode="drop")
    slot_live = jnp.zeros((ep_count * capacity,), jnp.int32).at[target].set(1, mode="drop")
    outgoing = jnp.where(slot_live[:, None] > 0, normed[slot_token], jnp.zeros((), jnp.bfloat16))
    outgoing = outgoing.reshape(ep_count, capacity, D)
    gate_slice = expert_gate[0]
    up_slice = expert_up[0]
    down_slice = expert_down[0]
    arrived = lax.all_to_all(outgoing, "ep", split_axis=0, concat_axis=0, tiled=True)
    gate_val = jnp.einsum("sid,df->sif", arrived, gate_slice, preferred_element_type=jnp.float32)
    up_val = jnp.einsum("sid,df->sif", arrived, up_slice, preferred_element_type=jnp.float32)
    hidden = (jax.nn.silu(gate_val) * up_val).astype(jnp.bfloat16)
    partial_value = jnp.einsum(
        "sif,fd->sid", hidden, down_slice, preferred_element_type=jnp.float32
    )
    partial_value = partial_value.astype(jnp.bfloat16)
    returned = lax.all_to_all(partial_value, "ep", split_axis=0, concat_axis=0, tiled=True)
    flat_back = returned.reshape(ep_count * capacity, returned.shape[2])
    gather_at = jnp.where(in_team, target, 0).reshape(tokens, top_count)
    weight_at = jnp.where(in_team, route_weights.reshape(-1), 0.0).reshape(tokens, top_count)
    combined = jnp.zeros((tokens, returned.shape[2]), jnp.float32)
    for pick_index in range(top_count):
        combined = (
            combined
            + flat_back[gather_at[:, pick_index]].astype(jnp.float32)
            * weight_at[:, pick_index][:, None]
        )
    shared_gate_val = jnp.dot(normed, shared_gate, preferred_element_type=jnp.float32)
    shared_up_val = jnp.dot(normed, shared_up, preferred_element_type=jnp.float32)
    shared_act = (jax.nn.silu(shared_gate_val) * shared_up_val).astype(jnp.bfloat16)
    return combined + jnp.dot(shared_act, shared_down, preferred_element_type=jnp.float32)


def shards(
    queries,
    key_vectors,
    values,
    out_gate,
    input_gate,
    forget_gate,
    mix_weight,
    expert_input,
    norm_gain,
    route_ids,
    route_weights,
    expert_gate,
    expert_up,
    expert_down,
    shared_gate,
    shared_up,
    shared_down,
):
    mixer_partial = mixer_half(
        queries, key_vectors, values, out_gate, input_gate, forget_gate, mix_weight
    )
    expert_partial = expert_half(
        expert_input,
        norm_gain,
        route_ids,
        route_weights,
        expert_gate,
        expert_up,
        expert_down,
        shared_gate,
        shared_up,
        shared_down,
    )
    mixer_piece = lax.psum_scatter(
        mixer_partial.astype(jnp.bfloat16), "tp", scatter_dimension=0, tiled=True
    )
    mixer_out = lax.all_gather(mixer_piece, "tp", axis=0, tiled=True)
    expert_piece = lax.psum_scatter(expert_partial, "tp", scatter_dimension=0, tiled=True).astype(
        jnp.bfloat16
    )
    expert_out = lax.all_gather(expert_piece, "tp", axis=0, tiled=True)
    return (mixer_out, expert_out)


def solution(mesh):
    return jax.shard_map(
        shards,
        mesh=mesh,
        in_specs=(
            P("ep", None),
            P("ep", None),
            P("ep", "tp"),
            P("ep", "tp"),
            P("ep", None),
            P("ep", None),
            P("tp", None),
            P("ep", None),
            P(),
            P("ep", None),
            P("ep", None),
            P(("ep", "tp"), None, None),
            P(("ep", "tp"), None, None),
            P(("ep", "tp"), None, None),
            P(None, "tp"),
            P(None, "tp"),
            P("tp", None),
        ),
        out_specs=(P("ep", None), P("ep", None)),
        check_vma=False,
    )
```

profile of v0, /device:TPU:1, one launch (start us, length us, event | category | flops | bytes accessed | tf_op | source)
XLA Modules:
  0.0 616.7 jit_solution(1964021302726074480)
XLA Ops:
  8.0 1.0 copy.27
  9.3 2.3 reduce-window.6
  12.4 4.3 scatter_custom_fusion.1
  17.1 4.3 scatter_custom_fusion
  21.8 11.0 %gather_fusion = bf16[2048,2048]{1,0:T(8,128)(2,1)} fusion(bf16[256,2048]{1,0:T(8,128)(2,1)S(1)} %fusion.3, s32[2048]{0:T(1024)S(1)} %fusion.51), kind=kCustom, calls=%fused_computation | custom fusion | bytes 16785408 | tf_op jit(solution)/shard_map/gather | solution.py:175
  32.8 7.2 %broadcast_select_fusion = bf16[8,256,2048]{2,1,0:T(8,128)(2,1)} fusion(bf16[8,256,2048]{2,1,0:T(8,128)(2,1)} %bitcast.111, pred[8,256]{1,0:T(8,128)(4,1)S(1)} %broadcast_in_dim.84), kind=kLoop, calls=%fused_computation.11 | loop fusion | flops 4194304 | bytes 16779264 | tf_op jit(solution)/shard_map/jit(_where)/select_n | solution.py:175
  40.0 188.6 %all_to_all.10 = bf16[8,256,2048]{2,1,0:T(8,128)(2,1)S(1)} all-to-all(bf16[8,256,2048]{2,1,0:T(8,128)(2,1)} %broadcast_select_fusion), channel_id=1, replica_groups=mesh['ep'=8,'tp'=4] {'ep'}, dimensions={0} | all-to-all | bytes 16777216 | tf_op jit(solution)/shard_map/all_to_all | solution.py:180
  228.6 3.2 copy-done.2
  231.9 3.8 fusion.16
  235.7 16.8 %convolution_convert_fusion = bf16[8,256,2048]{2,1,0:T(8,128)(2,1)} fusion(f32[8,256,256]{2,1,0:T(8,128)} %fusion.16, bf16[8,256,2048]{2,1,0:T(8,128)(2,1)} %copy-done.2, bf16[1,256,2048]{2,1,0:T(8,128)(2,1)S(1)} %copy-done, bf16[1,2048,256]{2,1,0:T(8,128)(2,1)} %param.30), kind=kOutput, calls=%fused_computation.12 | convolution fusion | flops 4302307328 | bytes 20971520 | tf_op jit(solution)/shard_map/sif,fd->sid/dot_general | solution.py:184
  252.5 5.1 all-to-all-start.1
  258.2 0.6 slice.33
  259.4 1.2 fusion.72
  262.0 1.3 subtract_exponential_fusion.1
  263.3 1.1 fusion.4
  265.1 1.3 bitcast_dynamic-update-slice_fusion
  266.4 0.8 dynamic-update-slice.1
  267.1 160.9 %all-reduce.2 = (f32[8]{0:T(128)S(1)}, f32[8]{0:T(128)S(1)}) all-reduce(f32[8]{0:T(128)S(1)} %bitcast_dynamic-update-slice_fusion, f32[8]{0:T(128)S(1)} %dynamic-update-slice.1), channel_id=2, replica_groups=mesh['ep'=8,'tp'=4] {'ep'}, use_global_device_ids=true, to_apply=%add | all-reduce | flops 16 | bytes 128 | tf_op jit(solution)/shard_map/all_gather | solution.py:20
  428.3 59.1 %all-gather.3 = f32[8,1,256]{2,1,0:T(1,128)S(1)} all-gather(f32[1,1,256]{2,1,0:T(1,128)S(1)} %bitcast.122), channel_id=4, replica_groups=mesh['ep'=8,'tp'=4] {'ep'}, dimensions={0}, use_global_device_ids=true | all-gather | bytes 9216 | tf_op jit(solution)/shard_map/all_gather | solution.py:20
  488.7 6.8 %gather_fusion.1 = bf16[256,2048]{1,0:T(8,128)(2,1)S(1)} fusion(bf16[2048,2048]{1,0:T(8,128)(2,1)} %bitcast.20, s32[1024]{0:T(1024)S(1)} %get-tuple-element.324), kind=kCustom, calls=%fused_computation.1 | custom fusion | bytes 2098176 | tf_op jit(solution)/shard_map/gather | solution.py:196
  495.5 7.8 %gather_fusion.2 = bf16[256,2048]{1,0:T(8,128)(2,1)} fusion(bf16[2048,2048]{1,0:T(8,128)(2,1)} %bitcast.20, s32[1024]{0:T(1024)S(1)} %get-tuple-element.323), kind=kCustom, calls=%fused_computation.2 | custom fusion | bytes 2098176 | tf_op jit(solution)/shard_map/gather | solution.py:196
  503.3 7.9 %gather_fusion.3 = bf16[256,2048]{1,0:T(8,128)(2,1)} fusion(bf16[2048,2048]{1,0:T(8,128)(2,1)} %bitcast.20, s32[1024]{0:T(1024)S(1)} %get-tuple-element.322), kind=kCustom, calls=%fused_computation.3 | custom fusion | bytes 2098176 | tf_op jit(solution)/shard_map/gather | solution.py:196
  511.2 8.1 %gather_fusion.4 = bf16[256,2048]{1,0:T(8,128)(2,1)} fusion(bf16[2048,2048]{1,0:T(8,128)(2,1)} %bitcast.20, s32[1024]{0:T(1024)S(1)} %get-tuple-element.321), kind=kCustom, calls=%fused_computation.4 | custom fusion | bytes 2098176 | tf_op jit(solution)/shard_map/gather | solution.py:196
  519.3 4.7 convolution_add_fusion
  524.1 35.5 %while.5 = (s32[]{:T(128)}, f32[]{:T(128)}, f32[256,256]{1,0:T(8,128)S(1)}, f32[256]{0:T(256)S(1)}, f32[]{:T(128)}, /*index=5*/s32[]{:T(128)}, f32[8]{0:T(128)S(...) while((s32[]{:T(128)}, f32[]{:T(128)}, ...), condition=%wide.region_6.7_spmd.clone, body=%wide.region_5.6_spmd.clone.sunk | while | flops 328971 | bytes 791841 | solution.py:29
  525.4 0.6 dynamic_slice.101
  527.3 1.1 fusion.89
  530.4 0.6 dynamic_slice.101
  532.4 1.1 fusion.89
  534.3 0.6 dynamic_slice.100
  535.5 0.6 dynamic_slice.101
  537.5 1.1 fusion.89
  539.3 0.6 dynamic_slice.100
  540.6 0.6 dynamic_slice.101
  542.5 1.1 fusion.89
  545.6 0.6 dynamic_slice.101
  547.6 1.1 fusion.89
  550.7 0.6 dynamic_slice.101
  552.7 1.1 fusion.89
  555.8 0.6 dynamic_slice.101
  557.7 1.1 fusion.89
  560.7 1.1 convolution_convert_fusion.1
  561.9 1.9 convert_element_type.76
  563.8 23.1 %reduce-scatter.3.cloned.1.call-done = bf16[32,2048]{1,0:T(8,128)(2,1)} async-done(((bf16[128,2048]{1,0:T(8,128)(2,1)}), bf16[32,2048]{1,0:T(8,128)(2,1)}) %reduce-scatter.3.cloned.1.call-update) | async-done | bytes 131088 | tf_op jit(solution)/shard_map/reduce_scatter | solution.py:239
  586.8 7.5 %all_gather.32 = bf16[128,2048]{1,0:T(8,128)(2,1)S(1)} all-gather(bf16[32,2048]{1,0:T(8,128)(2,1)} %reduce-scatter.3.cloned.1.call-done), channel_id=1, replica_groups=mesh['ep'=8,'tp'=4] {'tp'}, dimensions={0}, use_global_device_ids=true | all-gather | bytes 655360 | tf_op jit(solution)/shard_map/all_gather | solution.py:242
  594.3 11.7 %all-gather.7.cloned.1.call-done = bf16[256,2048]{1,0:T(8,128)(2,1)} async-done(((bf16[64,2048]{1,0:T(8,128)(2,1)}), bf16[256,2048]{1,0:T(8,128)(2,1)}) %all-gather.7.cloned.1.call-update) | async-done | bytes 1048592 | tf_op jit(solution)/shard_map/all_gather | solution.py:246
  606.0 0.8 copy.61
  606.8 2.3 copy.62
  (108 shorter events, 8.6 us)
Async XLA Ops:
  8.0 227.7 %copy-start = (bf16[1,256,2048]{2,1,0:T(8,128)(2,1)S(1)}, bf16[1,256,2048]{2,1,0:T(8,128)(2,1)}, u32[]{:S(2)}) copy-start(bf16[1,256,2048]{2,1,0:T(8,128)(2,1)} %param.32) | copy-start | bytes 3145732
  8.0 8.8 %copy-start.3 = (bf16[256,2048]{1,0:T(8,128)(2,1)S(1)}, bf16[256,2048]{1,0:T(8,128)(2,1)}, u32[]{:S(2)}) copy-start(bf16[256,2048]{1,0:T(8,128)(2,1)} %param.26) | copy-start | bytes 3145732
  8.0 13.4 %copy-start.10 = (f32[2048]{0:T(1024)S(1)}, f32[2048]{0:T(1024)}, u32[]{:S(2)}) copy-start(f32[2048]{0:T(1024)} %param.27) | copy-start | bytes 24580
  40.0 191.9 %copy-start.14 = (bf16[1,2048,256]{2,1,0:T(8,128)(2,1)S(1)}, bf16[1,2048,256]{2,1,0:T(8,128)(2,1)}, u32[]{:S(2)}) copy-start(bf16[1,2048,256]{2,1,0:T(8,128)(2,1)} %param.31) | copy-start | bytes 3145732
  228.6 3.2 copy-start.2
  252.5 5.2 copy-start.12
  252.5 5.2 copy-start.13
  252.5 10.8 %copy-start.7 = (bf16[128,256]{1,0:T(8,128)(2,1)S(1)}, bf16[128,256]{1,0:T(8,128)(2,1)}, u32[]{:S(2)}) copy-start(bf16[128,256]{1,0:T(8,128)(2,1)} %param.21) | copy-start | bytes 196612
  252.5 10.8 %copy-start.8 = (bf16[128,512]{1,0:T(8,128)(2,1)S(1)}, bf16[128,512]{1,0:T(8,128)(2,1)}, u32[]{:S(2)}) copy-start(bf16[128,512]{1,0:T(8,128)(2,1)} %param.20) | copy-start | bytes 393220
  252.5 12.0 %copy-start.16 = (u32[32]{0:T(128)S(1)}, u32[32]{0:T(128)}, u32[]{:S(2)}) copy-start(u32[32]{0:T(128)} %constant.182) | copy-start | bytes 388
  252.5 175.5 %copy-start.11 = (f32[256,4]{0,1:T(4,128)S(1)}, f32[256,4]{0,1:T(4,128)}, u32[]{:S(2)}) copy-start(f32[256,4]{0,1:T(4,128)} %param.29) | copy-start | bytes 12292
  252.5 236.1 %all-to-all-start.1 = ((bf16[8,256,2048]{2,1,0:T(8,128)(2,1)}), bf16[8,256,2048]{2,1,0:T(8,128)(2,1)}, u32[]{:S(2)}, u32[]{:S(2)}) async-start(bf16[8,256,2048]{2,1,0:T(8,128)(2,1)} %convolution_convert_fusion), calls=%async_computation.2 | async-start | bytes 16777216 | tf_op jit(solution)/shard_map/all_to_all | solution.py:188
  257.7 230.6 %copy-start.5 = (bf16[2048,128]{1,0:T(8,128)(2,1)S(1)}, bf16[2048,128]{1,0:T(8,128)(2,1)}, u32[]{:S(2)}) copy-start(bf16[2048,128]{1,0:T(8,128)(2,1)} %param.33) | copy-start | bytes 1572868
  257.7 266.4 %all-gather.9.cloned.1.call-start = ((), (), s32[]{:S(2)}) async-start(), calls=%async_computation.7 | async-start | bytes 2359296 | tf_op jit(solution)/shard_map/all_gather | solution.py:20
  264.4 297.5 %reduce-scatter.5.cloned.1.call-start = ((), (), s32[]{:S(2)}) async-start(), calls=%async_computation.5 | async-start | bytes 2621440 | tf_op jit(solution)/shard_map/reduce_scatter | solution.py:243
  511.2 8.1 %copy-start.6 = (bf16[128,2048]{1,0:T(8,128)(2,1)S(1)}, bf16[128,2048]{1,0:T(8,128)(2,1)}, u32[]{:S(2)}) copy-start(bf16[128,2048]{1,0:T(8,128)(2,1)} %param.35) | copy-start | bytes 1572868
  519.2 40.5 %copy-start.9 = (bf16[128,512]{1,0:T(8,128)(2,1)S(1)}, bf16[128,512]{1,0:T(8,128)(2,1)}, u32[]{:S(2)}) copy-start(bf16[128,512]{1,0:T(8,128)(2,1)} %param.19) | copy-start | bytes 393220
  524.0 62.8 %reduce-scatter.3.cloned.1.call-start = ((), (), s32[]{:S(2)}) async-start(), calls=%async_computation.4 | async-start | bytes 655360 | tf_op jit(solution)/shard_map/reduce_scatter | solution.py:239
  524.1 36.3 %copy-start.15 = (bf16[128,256]{1,0:T(8,128)(2,1)S(1)}, bf16[128,256]{1,0:T(8,128)(2,1)}, u32[]{:S(2)}) copy-start(bf16[128,256]{1,0:T(8,128)(2,1)} %param.22) | copy-start | bytes 196612
  524.1 36.6 %copy-start.4 = (bf16[256,2048]{1,0:T(8,128)(2,1)S(1)}, bf16[256,2048]{1,0:T(8,128)(2,1)}, u32[]{:S(2)}) copy-start(bf16[256,2048]{1,0:T(8,128)(2,1)} %param.25) | copy-start | bytes 3145732
  561.8 44.2 %all-gather.7.cloned.1.call-start = ((), (), s32[]{:S(2)}) async-start(), calls=%async_computation.6 | async-start | bytes 1310720 | tf_op jit(solution)/shard_map/all_gather | solution.py:246
  561.9 47.3 %copy-start.1 = (bf16[1,256,2048]{2,1,0:T(8,128)(2,1)S(1)}, bf16[1,256,2048]{2,1,0:T(8,128)(2,1)}, u32[]{:S(2)}) copy-start(bf16[1,256,2048]{2,1,0:T(8,128)(2,1)} %param.32) | copy-start | bytes 3145732
Sparse Core Ops, SparseCore 0:
  264.5 166.7 all-gather.8
Sparse Core Ops, SparseCore 1:
  524.1 34.4 reduce-scatter.4
  561.9 24.9 reduce-scatter.2
  588.8 17.1 all-gather.6
where the time goes:
time: 618 us; the launch traced here: 617 us
  blocking collectives  416 us (67%)
  local copies, waits for them, and re-layouts  70.3 us (11%)
  waiting for transfers between devices  34.9 us (6%)
  matrix products  28.9 us (5%)
  other arithmetic  24 us (4%)
  loops' own time  19.1 us (3%)
  between operations  18.2 us (3%)
    all_gather x2, blocking collectives, prefix_2(): pieces = jax.tree.map(lambda part: lax.all_gather(part, axis), value)  220 us
    all_to_all x1, blocking collectives, expert_half(): lax.all_to_all(outgoing, 'ep', split_axis=0, concat_axis=0, tiled=True)  189 us
    gather x4, local copies, waits for them, and re-layouts, expert_half(): flat_back[gather_at[:, pick_index]].astype(jnp.float32)  30.6 us
    reduce_scatter x1, waiting for transfers between devices, shards(): lax.psum_scatter(mixer_partial.astype(jnp.bfloat16), 'tp', scatter_dimens...  23.1 us
    another operation x1, loops' own time, prefix_2(): return lax.fori_loop(0, count - 1, turn, subtotal)  19.1 us
    dot_general x1, matrix products, expert_half(): jnp.einsum('sif,fd->sid', hidden, down_slice, preferred_element_type=jnp....  16.8 us
  transfers between devices with their start and end apart: 5, of which 2 were waited for; matrix products, arithmetic and copies ran while one was open for 10% of the time, Pallas kernels for 0%

commit v1 on v0

v1 whole, which is shorter than its diff:
```python
import jax
import jax.numpy as jnp
from jax import lax
from jax.sharding import PartitionSpec as P

D = 2048
MEMORY_HEADS = 2
KEY_DIM = 256
BLOCK = 128
FF = 1024


epsilon = 1e-06
lowest = -1e30
den_floor = 4.0


def mixer_half(queries, key_vectors, values, out_gate, input_gate, forget_gate, mix_weight):
    tp_count = lax.axis_size("tp")
    tp_rank = lax.axis_index("tp")
    ep_count = lax.axis_size("ep")
    ep_rank = lax.axis_index("ep")
    length = queries.shape[0]
    channels = values.shape[1]
    factor = KEY_DIM ** (-0.5)
    head_index = tp_rank // (tp_count // MEMORY_HEADS)
    offset = head_index * KEY_DIM
    query_head = lax.dynamic_slice_in_dim(queries, offset, KEY_DIM, 1)
    key_head = lax.dynamic_slice_in_dim(key_vectors, offset, KEY_DIM, 1)
    both = lax.all_gather(jnp.concatenate([key_head, values], axis=1), "ep", axis=0, tiled=True)
    keys_all = both[:, :KEY_DIM]
    values_all = both[:, KEY_DIM:]
    select = jnp.arange(MEMORY_HEADS, dtype=jnp.int32)[None, :] == head_index
    gates = jnp.stack(
        [
            jnp.sum(jnp.where(select, input_gate, 0.0), axis=1),
            jax.nn.log_sigmoid(jnp.sum(jnp.where(select, forget_gate, 0.0), axis=1)),
        ]
    )
    gates = lax.all_gather(gates, "ep", axis=1, tiled=True)
    total = ep_count * length
    blocks = total // BLOCK
    mine = length // BLOCK
    input_all = gates[0].reshape(blocks, BLOCK)
    cumulative = jnp.cumsum(gates[1].reshape(blocks, BLOCK), axis=1)
    block_total = cumulative[:, -1]
    index = jnp.arange(blocks, dtype=jnp.int32)
    here = ep_rank * mine + jnp.arange(mine, dtype=jnp.int32)
    between = (index[None, None, :] > index[None, :, None]) & (
        index[None, None, :] < here[:, None, None]
    )
    gap = jnp.sum(jnp.where(between, block_total[None, None, :], 0.0), axis=2)
    ahead = jnp.sum(jnp.where(index[None, :] < here[:, None], block_total[None, :], 0.0), axis=1)
    keep = block_total[:, None] - cumulative + input_all
    own_cumulative = lax.dynamic_slice_in_dim(cumulative, ep_rank * mine, mine, 0)
    same = index[None, :] == here[:, None]
    column = jnp.where(same[:, :, None], input_all - cumulative, keep + gap[:, :, None])
    log_weight = own_cumulative[:, :, None, None] + column[:, None]
    row_at = jnp.arange(BLOCK, dtype=jnp.int32)
    visible = (index[None, :] < here[:, None])[:, None, :, None] | (
        same[:, None, :, None] & (row_at[None, :, None, None] >= row_at[None, None, None, :])
    )
    log_weight = jnp.where(visible, log_weight, -jnp.inf).reshape(length, total)
    carried = (own_cumulative + ahead[:, None]).reshape(length)
    stabilizer = jnp.maximum(carried, jnp.max(log_weight, axis=1))
    within = jnp.exp(log_weight - stabilizer[:, None])
    scores = (
        jnp.einsum("td,sd->ts", query_head, keys_all, preferred_element_type=jnp.float32) * factor
    )
    weights = scores * within
    numerator = jnp.dot(
        weights.astype(jnp.bfloat16), values_all, preferred_element_type=jnp.float32
    )
    denominator = jnp.sum(weights, axis=1)
    hidden = numerator / jnp.maximum(jnp.abs(denominator), den_floor)[:, None]
    gated_rows = (hidden * jax.nn.sigmoid(out_gate.astype(jnp.float32))).astype(jnp.bfloat16)
    return jnp.dot(gated_rows, mix_weight, preferred_element_type=jnp.float32)


def dense_experts(
    expert_input,
    norm_gain,
    route_ids,
    route_weights,
    expert_gate,
    expert_up,
    expert_down,
    shared_gate,
    shared_up,
    shared_down,
):
    ep_count = lax.axis_size("ep")
    tp_count = lax.axis_size("tp")
    tp_rank = lax.axis_index("tp")
    ep_rank = lax.axis_index("ep")
    tokens = expert_input.shape[0]
    share = tokens // tp_count
    rows_wide = expert_input.astype(jnp.float32)
    normed = (
        rows_wide
        * lax.rsqrt(jnp.mean(rows_wide * rows_wide, axis=-1, keepdims=True) + epsilon)
        * norm_gain
    ).astype(jnp.bfloat16)
    part = lax.dynamic_slice_in_dim(normed, tp_rank * share, share, 0)
    everyone = lax.all_gather(part, ("ep", "tp"), axis=0, tiled=True)
    named = route_ids[:, :, None] == jnp.arange(ep_count, dtype=jnp.int32)[None, None, :]
    table = jnp.sum(jnp.where(named, route_weights[:, :, None], 0.0), axis=1).T
    table = lax.all_to_all(table, "ep", split_axis=0, concat_axis=1, tiled=True)
    mine = table.reshape(ep_count * tokens)
    gate_val = jnp.dot(everyone, expert_gate[0], preferred_element_type=jnp.float32)
    up_val = jnp.dot(everyone, expert_up[0], preferred_element_type=jnp.float32)
    hidden = (jax.nn.silu(gate_val) * up_val).astype(jnp.bfloat16)
    partial_value = jnp.dot(hidden, expert_down[0], preferred_element_type=jnp.float32)
    partial_value = (partial_value * mine[:, None]).astype(jnp.bfloat16)
    routed = lax.psum_scatter(partial_value, ("ep", "tp"), scatter_dimension=0, tiled=True)
    shared_gate_val = jnp.dot(normed, shared_gate, preferred_element_type=jnp.float32)
    shared_up_val = jnp.dot(normed, shared_up, preferred_element_type=jnp.float32)
    shared_act = (jax.nn.silu(shared_gate_val) * shared_up_val).astype(jnp.bfloat16)
    shared = jnp.dot(shared_act, shared_down, preferred_element_type=jnp.float32)
    shared = lax.psum_scatter(
        shared.astype(jnp.bfloat16), "tp", scatter_dimension=0, tiled=True
    )
    piece = (routed.astype(jnp.float32) + shared.astype(jnp.float32)).astype(jnp.bfloat16)
    return lax.all_gather(piece, "tp", axis=0, tiled=True)


def expert_half(
    expert_input,
    norm_gain,
    route_ids,
    route_weights,
    expert_gate,
    expert_up,
    expert_down,
    shared_gate,
    shared_up,
    shared_down,
):
    ep_count = lax.axis_size("ep")
    tp_count = lax.axis_size("tp")
    tp_rank = lax.axis_index("tp")
    tokens = expert_input.shape[0]
    top_count = route_ids.shape[1]
    slice_units = expert_gate.shape[2]
    group_size = FF // slice_units
    per_ep = tp_count // group_size
    team_index = tp_rank // group_size
    expert_count = ep_count * per_ep
    capacity = 2 * tokens * top_count // expert_count
    rows_wide = expert_input.astype(jnp.float32)
    normed = (
        rows_wide
        * lax.rsqrt(jnp.mean(rows_wide * rows_wide, axis=-1, keepdims=True) + epsilon)
        * norm_gain
    ).astype(jnp.bfloat16)
    chosen = route_ids.reshape(-1)
    onehot = (chosen[:, None] == jnp.arange(expert_count, dtype=jnp.int32)[None, :]).astype(
        jnp.int32
    )
    slot_rank = jnp.sum((jnp.cumsum(onehot, axis=0) - onehot) * onehot, axis=1)
    in_team = chosen % per_ep == team_index
    target = jnp.where(in_team, chosen // per_ep * capacity + slot_rank, ep_count * capacity)
    token_of = jnp.arange(chosen.shape[0], dtype=jnp.int32) // top_count
    slot_token = jnp.zeros((ep_count * capacity,), jnp.int32).at[target].set(token_of, mode="drop")
    slot_live = jnp.zeros((ep_count * capacity,), jnp.int32).at[target].set(1, mode="drop")
    outgoing = jnp.where(slot_live[:, None] > 0, normed[slot_token], jnp.zeros((), jnp.bfloat16))
    outgoing = outgoing.reshape(ep_count, capacity, D)
    gate_slice = expert_gate[0]
    up_slice = expert_up[0]
    down_slice = expert_down[0]
    arrived = lax.all_to_all(outgoing, "ep", split_axis=0, concat_axis=0, tiled=True)
    gate_val = jnp.einsum("sid,df->sif", arrived, gate_slice, preferred_element_type=jnp.float32)
    up_val = jnp.einsum("sid,df->sif", arrived, up_slice, preferred_element_type=jnp.float32)
    hidden = (jax.nn.silu(gate_val) * up_val).astype(jnp.bfloat16)
    partial_value = jnp.einsum(
        "sif,fd->sid", hidden, down_slice, preferred_element_type=jnp.float32
    )
    partial_value = partial_value.astype(jnp.bfloat16)
    returned = lax.all_to_all(partial_value, "ep", split_axis=0, concat_axis=0, tiled=True)
    flat_back = returned.reshape(ep_count * capacity, returned.shape[2])
    gather_at = jnp.where(in_team, target, 0).reshape(tokens, top_count)
    weight_at = jnp.where(in_team, route_weights.reshape(-1), 0.0).reshape(tokens, top_count)
    combined = jnp.zeros((tokens, returned.shape[2]), jnp.float32)
    for pick_index in range(top_count):
        combined = (
            combined
            + flat_back[gather_at[:, pick_index]].astype(jnp.float32)
            * weight_at[:, pick_index][:, None]
        )
    shared_gate_val = jnp.dot(normed, shared_gate, preferred_element_type=jnp.float32)
    shared_up_val = jnp.dot(normed, shared_up, preferred_element_type=jnp.float32)
    shared_act = (jax.nn.silu(shared_gate_val) * shared_up_val).astype(jnp.bfloat16)
    return combined + jnp.dot(shared_act, shared_down, preferred_element_type=jnp.float32)


def shards(
    queries,
    key_vectors,
    values,
    out_gate,
    input_gate,
    forget_gate,
    mix_weight,
    expert_input,
    norm_gain,
    route_ids,
    route_weights,
    expert_gate,
    expert_up,
    expert_down,
    shared_gate,
    shared_up,
    shared_down,
):
    ep_count, tp_count = lax.axis_size("ep"), lax.axis_size("tp")
    tokens, slots = expert_input.shape[0], route_ids.shape[1] * 2 * expert_input.shape[0]
    per_ep = tp_count * expert_gate.shape[2] // FF
    dense = per_ep == 1 and slots // (ep_count * per_ep) >= tokens
    mixer_partial = mixer_half(
        queries, key_vectors, values, out_gate, input_gate, forget_gate, mix_weight
    )
    experts = dense_experts if dense else expert_half
    expert_partial = experts(
        expert_input,
        norm_gain,
        route_ids,
        route_weights,
        expert_gate,
        expert_up,
        expert_down,
        shared_gate,
        shared_up,
        shared_down,
    )
    mixer_piece = lax.psum_scatter(
        mixer_partial.astype(jnp.bfloat16), "tp", scatter_dimension=0, tiled=True
    )
    mixer_out = lax.all_gather(mixer_piece, "tp", axis=0, tiled=True)
    if dense:
        return (mixer_out, expert_partial)
    expert_piece = lax.psum_scatter(expert_partial, "tp", scatter_dimension=0, tiled=True).astype(
        jnp.bfloat16
    )
    expert_out = lax.all_gather(expert_piece, "tp", axis=0, tiled=True)
    return (mixer_out, expert_out)


def solution(mesh):
    return jax.shard_map(
        shards,
        mesh=mesh,
        in_specs=(
            P("ep", None),
            P("ep", None),
            P("ep", "tp"),
            P("ep", "tp"),
            P("ep", None),
            P("ep", None),
            P("tp", None),
            P("ep", None),
            P(),
            P("ep", None),
            P("ep", None),
            P(("ep", "tp"), None, None),
            P(("ep", "tp"), None, None),
            P(("ep", "tp"), None, None),
            P(None, "tp"),
            P(None, "tp"),
            P("tp", None),
        ),
        out_specs=(P("ep", None), P("ep", None)),
        check_vma=False,
    )
```

time: 618 us -> 315 us (0.51)
  blocking collectives: 416 us -> 23.5 us
  waiting for transfers between devices: 34.9 us -> 225 us
  local copies, waits for them, and re-layouts: 70.3 us -> 5.63 us
  loops' own time: 19.1 us -> 0 us
  other arithmetic: 24 us -> 9.5 us
    all_gather x2 -> x1, blocking collectives: 220 us -> 16.1 us  [mixer_half(): gates = lax.all_gather(gates, 'ep', axis=1, tiled=True)]
    all_to_all x1 -> x0, blocking collectives: 189 us -> none  [expert_half(): lax.all_to_all(outgoing, 'ep', split_axis=0, concat_axis=0, tiled=True)]
    reduce_scatter x1 -> x2, waiting for transfers between devices: 0.02 us -> 120 us  [the longest x1 120 us: dense_experts(): lax.psum_scatter(partial_value, ('ep', 'tp'), scatter_dimension=0, tiled=...]
    all_gather x2 -> x3, waiting for transfers between devices: 11.8 us -> 80.4 us  [the longest x1 68.5 us: dense_experts(): everyone = lax.all_gather(part, ('ep', 'tp'), axis=0, tiled=True)]
    gather x5 -> x0, local copies, waits for them, and re-layouts: 41.6 us -> none  [the longest x4 30.6 us: expert_half(): flat_back[gather_at[:, pick_index]].astype(jnp.float32)]
    another operation x1 -> x0, loops' own time: 19.1 us -> none  [prefix_2(): return lax.fori_loop(0, count - 1, turn, subtotal)]
    select_n x20 -> x2, other arithmetic: 15.7 us -> 0.15 us  [mixer_half(): jnp.where(same[:, :, None], input_all - cumulative, keep + gap[:, :, None])]
    scatter x2 -> x0, local copies, waits for them, and re-layouts: 8.63 us -> none  [the longest x1 4.32 us: expert_half(): jnp.zeros((ep_count * capacity,), jnp.int32).at[target]]
  transfers between devices with their start and end apart: 5 -> 7, of which waited for: 2 -> 4; matrix products, arithmetic and copies ran while one was open for 10% -> 11% of each run, Pallas kernels for 0% -> 0%
where the time goes in v1:
time: 315 us; the launch traced here: 314 us
  waiting for transfers between devices  225 us (71%)
  matrix products  28.4 us (9%)
  blocking collectives  23.5 us (7%)
  between operations  16 us (5%)
  other arithmetic  9.5 us (3%)
  starting transfers between devices  6.6 us (2%)
  local copies, waits for them, and re-layouts  5.63 us (2%)
    reduce_scatter x1, waiting for transfers between devices, dense_experts(): lax.psum_scatter(partial_value, ('ep', 'tp'), scatter_dimension=0, tiled=...  120 us
    all_gather x1, waiting for transfers between devices, dense_experts(): everyone = lax.all_gather(part, ('ep', 'tp'), axis=0, tiled=True)  68.5 us
    reduce_scatter x1, waiting for transfers between devices, shards(): lax.psum_scatter(mixer_partial.astype(jnp.bfloat16), 'tp', scatter_dimens...  23.9 us
    all_gather x1, blocking collectives, mixer_half(): gates = lax.all_gather(gates, 'ep', axis=1, tiled=True)  16.1 us
    dot_general x1, matrix products, dense_experts(): jnp.dot(hidden, expert_down[0], preferred_element_type=jnp.float32)  13.3 us
    all_gather x1, waiting for transfers between devices, dense_experts(): return lax.all_gather(piece, 'tp', axis=0, tiled=True)  11.9 us
    all_gather x1, blocking collectives, shards(): mixer_out = lax.all_gather(mixer_piece, 'tp', axis=0, tiled=True)  7.48 us
    dot_general x1, matrix products, dense_experts(): jnp.dot(everyone, expert_gate[0], preferred_element_type=jnp.float32)  7.32 us
  transfers between devices with their start and end apart: 7, of which 4 were waited for; matrix products, arithmetic and copies ran while one was open for 11% of the time, Pallas kernels for 0%

profile of v1, /device:TPU:1, one launch (start us, length us, event | category | flops | bytes accessed | tf_op | source)
XLA Modules:
  0.0 314.3 jit_solution(4326463726185072554)
XLA Ops:
  8.0 0.0 all-gather.6.cloned.1.call-start
  8.1 1.6 fusion.1
  9.7 1.6 fusion.3
  11.3 0.7 constant_dynamic-slice_fusion
  12.1 0.0 all-gather.6.cloned.1.call-update
  12.1 0.0 all-gather.4.cloned.1.call-start
  12.2 0.7 pad_maximum_fusion
  12.9 0.0 reduce-scatter.8.cloned.1.call-start
  12.9 1.5 fusion.51
  14.4 1.8 convolution_convert_fusion
  16.2 0.0 reduce-scatter.8.cloned.1.call-update
  16.3 0.6 copy.25
  16.9 6.3 %all-to-all-start = ((f32[8,1,256]{2,1,0:T(1,128)}), f32[8,1,256]{2,1,0:T(1,128)S(1)}, u32[]{:S(2)}, u32[]{:S(2)}) async-start(f32[8,1,256]{2,1,0:T(1,128)} %copy.25), calls=%async_computation.1 | async-start | bytes 16384 | tf_op jit(solution)/shard_map/all_to_all | solution.py:108
  23.2 0.0 reduce-scatter.6.cloned.1.call-start
  23.3 68.5 %all-gather.6.cloned.1.call-done = bf16[2048,2048]{1,0:T(8,128)(2,1)} async-done(((bf16[64,2048]{1,0:T(8,128)(2,1)}), bf16[2048,2048]{1,0:T(8,128)(2,1)}) %all-gather.6.cloned.1.call-update) | async-done | bytes 8388624 | tf_op jit(solution)/shard_map/all_gather | solution.py:105
  91.8 7.3 %fusion.11 = f32[2048,256]{1,0:T(8,128)} fusion(bf16[2048,2048]{1,0:T(8,128)(2,1)} %all-gather.6.cloned.1.call-done, bf16[1,2048,256]{2,1,0:T(8,128)(2,1)} %param.28), kind=kOutput, calls=%fused_computation.19 | convolution fusion | flops 2147483648 | bytes 11534336 | tf_op jit(solution)/shard_map/dot_general | solution.py:110
  99.1 13.3 %multiply_convert_fusion = bf16[2048,2048]{1,0:T(8,128)(2,1)} fusion(f32[2048]{0:T(1024)S(1)} %bitcast.82, bf16[2048,2048]{1,0:T(8,128)(2,1)} %all-gather.6.cloned.1.call-done, f32[2048,256]{1,0:T(8,128)} %fusion.11, bf16[1,256,2048]{2,1,0:T(8,128)(2,1)S(1)} %copy-done, bf16[1,2048,256]{2,1,0:T(8,128)(2,1)S(1)} %copy-done.9), kind=kOutput, calls=%fused_computation | convolution fusion | flops 4306501632 | bytes 20979712 | tf_op jit(solution)/shard_map/dot_general | solution.py:113
  112.4 0.0 reduce-scatter.6.cloned.1.call-update
  112.5 0.0 reduce-scatter.4.cloned.1.call-start
  112.5 0.6 copy-done.7
  113.1 0.1 select_reduce_fusion.4
  113.2 16.1 %all_gather.16 = f32[2,1024]{1,0:T(2,128)S(1)} all-gather(f32[2,128]{1,0:T(2,128)S(1)} %pad_maximum_fusion.1), channel_id=1, replica_groups=mesh['ep'=8,'tp'=4] {'ep'}, dimensions={1}, use_global_device_ids=true | all-gather | bytes 9216 | tf_op jit(solution)/shard_map/all_gather | solution.py:40
  129.3 0.3 reduce_window_sum.13
  129.6 0.2 slice_reduce_fusion
  129.8 0.6 fusion.39
  130.4 0.1 select_reduce_fusion.2
  130.5 0.1 add_select_fusion
  130.6 1.9 select_reduce_fusion
  132.4 0.7 bitcast_maximum_fusion
  133.1 0.1 broadcast_bitcast_fusion.1
  133.2 0.1 broadcast_bitcast_fusion
  133.3 0.1 sub.45
  133.3 0.1 add.125
  133.4 0.1 fusion.34
  133.5 0.1 and.56
  133.6 2.2 fusion.50
  135.8 2.4 convolution_convert_fusion.1
  138.2 0.0 reduce-scatter.4.cloned.1.call-update
  138.2 0.0 all-gather.8.cloned.1.call-start
  138.2 0.0 reduce-scatter.8.cloned.1.call-done
  138.3 120.3 %reduce-scatter.6.cloned.1.call-done = bf16[64,2048]{1,0:T(8,128)(2,1)} async-done(((bf16[2048,2048]{1,0:T(8,128)(2,1)}), bf16[64,2048]{1,0:T(8,128)(2,1)}) %reduce-scatter.6.cloned.1.call-update) | async-done | bytes 262160 | tf_op jit(solution)/shard_map/reduce_scatter | solution.py:115
  258.6 1.8 add_convert_fusion
  260.4 0.0 all-gather.8.cloned.1.call-update
  260.4 23.9 %reduce-scatter.4.cloned.1.call-done = bf16[32,2048]{1,0:T(8,128)(2,1)} async-done(((bf16[128,2048]{1,0:T(8,128)(2,1)}), bf16[32,2048]{1,0:T(8,128)(2,1)}) %reduce-scatter.4.cloned.1.call-update) | async-done | bytes 131088 | tf_op jit(solution)/shard_map/reduce_scatter | solution.py:235
  284.3 7.5 %all_gather.17 = bf16[128,2048]{1,0:T(8,128)(2,1)S(1)} all-gather(bf16[32,2048]{1,0:T(8,128)(2,1)} %reduce-scatter.4.cloned.1.call-done), channel_id=1, replica_groups=mesh['ep'=8,'tp'=4] {'tp'}, dimensions={0}, use_global_device_ids=true | all-gather | bytes 655360 | tf_op jit(solution)/shard_map/all_gather | solution.py:238
  291.7 11.9 %all-gather.8.cloned.1.call-done = bf16[256,2048]{1,0:T(8,128)(2,1)} async-done(((bf16[64,2048]{1,0:T(8,128)(2,1)}), bf16[256,2048]{1,0:T(8,128)(2,1)}) %all-gather.8.cloned.1.call-update) | async-done | bytes 1048592 | tf_op jit(solution)/shard_map/all_gather | solution.py:124
  303.6 0.8 copy.30
  304.4 2.3 copy.31
  (41 shorter events, 0.2 us)
Async XLA Ops:
  8.0 91.1 %copy-start = (bf16[1,256,2048]{2,1,0:T(8,128)(2,1)S(1)}, bf16[1,256,2048]{2,1,0:T(8,128)(2,1)}, u32[]{:S(2)}) copy-start(bf16[1,256,2048]{2,1,0:T(8,128)(2,1)} %param.30) | copy-start | bytes 3145732
  8.0 4.2 %copy-start.4 = (bf16[128,512]{1,0:T(8,128)(2,1)S(1)}, bf16[128,512]{1,0:T(8,128)(2,1)}, u32[]{:S(2)}) copy-start(bf16[128,512]{1,0:T(8,128)(2,1)} %param.18) | copy-start | bytes 393220
  8.0 4.2 %copy-start.3 = (bf16[128,256]{1,0:T(8,128)(2,1)S(1)}, bf16[128,256]{1,0:T(8,128)(2,1)}, u32[]{:S(2)}) copy-start(bf16[128,256]{1,0:T(8,128)(2,1)} %param.19) | copy-start | bytes 196612
  8.0 83.7 %all-gather.6.cloned.1.call-start = ((), (), s32[]{:S(2)}) async-start(), calls=%async_computation.6 | async-start | bytes 8650752 | tf_op jit(solution)/shard_map/all_gather | solution.py:105
  9.7 4.7 %copy-start.1 = (bf16[128,2048]{1,0:T(8,128)(2,1)S(1)}, bf16[128,2048]{1,0:T(8,128)(2,1)}, u32[]{:S(2)}) copy-start(bf16[128,2048]{1,0:T(8,128)(2,1)} %param.33) | copy-start | bytes 1572868
  9.7 4.7 %copy-start.2 = (bf16[2048,128]{1,0:T(8,128)(2,1)S(1)}, bf16[2048,128]{1,0:T(8,128)(2,1)}, u32[]{:S(2)}) copy-start(bf16[2048,128]{1,0:T(8,128)(2,1)} %param.32) | copy-start | bytes 1572868
  12.1 121.4 %all-gather.4.cloned.1.call-start = ((), (), s32[]{:S(2)}) async-start(), calls=%async_computation.4 | async-start | bytes 1179648 | tf_op jit(solution)/shard_map/all_gather | solution.py:30
  12.9 125.4 %reduce-scatter.8.cloned.1.call-start = ((), (), s32[]{:S(2)}) async-start(), calls=%async_computation.8 | async-start | bytes 1310720 | tf_op jit(solution)/shard_map/reduce_scatter | solution.py:120
  14.4 1.8 copy-start.5
  14.4 1.8 copy-start.6
  16.9 82.2 %all-to-all-start = ((f32[8,1,256]{2,1,0:T(1,128)}), f32[8,1,256]{2,1,0:T(1,128)S(1)}, u32[]{:S(2)}, u32[]{:S(2)}) async-start(f32[8,1,256]{2,1,0:T(1,128)} %copy.25), calls=%async_computation.1 | async-start | bytes 16384 | tf_op jit(solution)/shard_map/all_to_all | solution.py:108
  23.2 75.9 %copy-start.9 = (bf16[1,2048,256]{2,1,0:T(8,128)(2,1)S(1)}, bf16[1,2048,256]{2,1,0:T(8,128)(2,1)}, u32[]{:S(2)}) copy-start(bf16[1,2048,256]{2,1,0:T(8,128)(2,1)} %param.29) | copy-start | bytes 3145732
  23.2 235.4 %reduce-scatter.6.cloned.1.call-start = ((), (), s32[]{:S(2)}) async-start(), calls=%async_computation.7 | async-start | bytes 8650752 | tf_op jit(solution)/shard_map/reduce_scatter | solution.py:115
  112.4 0.7 copy-start.7
  112.4 0.7 copy-start.8
  112.4 21.2 %copy-start.12 = (bf16[128,512]{1,0:T(8,128)(2,1)S(1)}, bf16[128,512]{1,0:T(8,128)(2,1)}, u32[]{:S(2)}) copy-start(bf16[128,512]{1,0:T(8,128)(2,1)} %param.17) | copy-start | bytes 393220
  112.4 23.3 %copy-start.10 = (bf16[256,2048]{1,0:T(8,128)(2,1)S(1)}, bf16[256,2048]{1,0:T(8,128)(2,1)}, u32[]{:S(2)}) copy-start(bf16[256,2048]{1,0:T(8,128)(2,1)} %param.23) | copy-start | bytes 3145732
  112.5 23.3 %copy-start.13 = (bf16[128,256]{1,0:T(8,128)(2,1)S(1)}, bf16[128,256]{1,0:T(8,128)(2,1)}, u32[]{:S(2)}) copy-start(bf16[128,256]{1,0:T(8,128)(2,1)} %param.20) | copy-start | bytes 196612
  112.5 171.8 %reduce-scatter.4.cloned.1.call-start = ((), (), s32[]{:S(2)}) async-start(), calls=%async_computation.5 | async-start | bytes 655360 | tf_op jit(solution)/shard_map/reduce_scatter | solution.py:235
  133.5 2.3 copy-start.11
  138.2 165.4 %all-gather.8.cloned.1.call-start = ((), (), s32[]{:S(2)}) async-start(), calls=%async_computation.9 | async-start | bytes 1310720 | tf_op jit(solution)/shard_map/all_gather | solution.py:124
Sparse Core Ops, SparseCore 0:
  12.3 79.4 all-gather.5
  93.9 37.2 all-gather.3
Sparse Core Ops, SparseCore 1:
  16.5 26.5 reduce-scatter.7
  112.5 146.0 reduce-scatter.5
  261.5 22.7 reduce-scatter.3
  286.4 17.1 all-gather.7

commit v2 on v1

--- a/solution.py
+++ b/solution.py
@@ -1,6 +1,10 @@
+import functools
+
 import jax
 import jax.numpy as jnp
 from jax import lax
+from jax.experimental import pallas as pl
+from jax.experimental.pallas import tpu as pltpu
 from jax.sharding import PartitionSpec as P
 
 D = 2048
@@ -74,10 +78,324 @@
     denominator = jnp.sum(weights, axis=1)
     hidden = numerator / jnp.maximum(jnp.abs(denominator), den_floor)[:, None]
     gated_rows = (hidden * jax.nn.sigmoid(out_gate.astype(jnp.float32))).astype(jnp.bfloat16)
-    return jnp.dot(gated_rows, mix_weight, preferred_element_type=jnp.float32)
+    return gated_rows
+
+
+def dense_kernel(
+    lines, teams, x_ref, wt_ref, sact_ref, gated_ref, g_ref, u_ref, d_ref, sd_ref, mw_ref,
+    eo_ref, mo_ref,
+    tok, act, dq, sdq, mwq, sall, gall, xout, xin, own, zout, zin, fin, mfin,
+    z_send, z_recv, x_send, x_recv, c_send, c_recv, a_send, a_recv,
+    w_send, w_recv, xo_send, xo_recv, zo_send, zo_recv, f_send, f_recv,
+):
+    me = lax.axis_index("ep")
+    j = lax.axis_index("tp")
+    z, x = me // 2, me % 2
+    half_rows = x_ref.shape[0] // 2
+    core = j % 2
+    buddy = j + 1 - 2 * core
+    quarter = fin.shape[2]
+    mine_rows = pl.ds(pl.multiple_of(core * half_rows, half_rows), half_rows)
+    other_rows = pl.ds(pl.multiple_of((1 - core) * half_rows, half_rows), half_rows)
+
+    def remote(src, dst, send, recv, ep, tp):
+        return pltpu.make_async_remote_copy(
+            src_ref=src, dst_ref=dst, send_sem=send, recv_sem=recv,
+            device_id={"ep": ep, "tp": tp}, device_id_type=pl.DeviceIdType.MESH,
+        )
+
+    barrier = pltpu.get_barrier_semaphore()
+
+    def greet(ep, tp):
+        pl.semaphore_signal(
+            barrier, inc=1, device_id={"ep": ep, "tp": tp}, device_id_type=pl.DeviceIdType.MESH
+        )
+
+    greet(z * 2 + 1 - x, j)
+    for k in range(1, lines):
+        greet(lax.rem(z + k, lines) * 2 + x, j)
+    for k in range(1, teams):
+        greet(me, lax.rem(j + k, teams))
+    pl.semaphore_wait(barrier, lines + teams - 1)
+
+    def columns(ref, q):
+        return ref.at[:, pl.ds(pl.multiple_of(q * quarter, quarter), quarter)]
+
+    def team_copies(k):
+        p = lax.rem(j + k, teams)
+        pairs = (
+            (sact_ref, sall.at[j]),
+            (columns(sd_ref, p), sdq.at[j]),
+            (gated_ref, gall.at[j]),
+            (columns(mw_ref, p), mwq.at[j]),
+            (columns(d_ref, p), dq.at[j]),
+        )
+        return [
+            remote(src, dst, w_send.at[n, k - 1], w_recv.at[n, k - 1], me, p)
+            for n, (src, dst) in enumerate(pairs)
+        ]
+
+    def z_copy(zb, way):
+        to = z + 1 - 2 * way
+        ref = tok.at[zb * 2 + x, mine_rows]
+        return remote(ref, ref, z_send.at[way, zb], z_recv.at[zb], to * 2 + x, j)
+
+    def x_copy(zb):
+        ref = tok.at[zb * 2 + x, mine_rows]
+        return remote(ref, ref, x_send.at[zb], x_recv.at[zb], z * 2 + 1 - x, j)
+
+    def x_arrival(zb):
+        ref = tok.at[zb * 2 + 1 - x, mine_rows]
+        return remote(ref, ref, x_send.at[zb], x_recv.at[zb], z * 2 + 1 - x, j)
+
+    def c_copy(block):
+        ref = tok.at[block, mine_rows]
+        return remote(ref, ref, c_send.at[block], c_recv.at[block], me, buddy)
+
+    def c_arrival(block):
+        ref = tok.at[block, other_rows]
+        return remote(ref, ref, c_send.at[block], c_recv.at[block], me, buddy)
+
+    def a_copy(block, k):
+        p = lax.rem(j + k, teams)
+        return remote(
+            act.at[block, j], act.at[block, j],
+            a_send.at[block, k - 1], a_recv.at[block, k - 1], me, p,
+        )
+
+    def a_arrival(block, k):
+        p = lax.rem(j + teams - k, teams)
+        return remote(
+            act.at[block, p], act.at[block, p],
+            a_send.at[block, k - 1], a_recv.at[block, k - 1], me, p,
+        )
+
+    tok[me] = x_ref[...]
+    for way in range(2):
+        to = z + 1 - 2 * way
+
+        @pl.when((to >= 0) & (to < lines))
+        def _():
+            remote(
+                x_ref.at[mine_rows], tok.at[me, mine_rows],
+                z_send.at[way, z], z_recv.at[z], to * 2 + x, j,
+            ).start()
+
+    remote(
+        x_ref.at[mine_rows], tok.at[me, mine_rows], x_send.at[z], x_recv.at[z], z * 2 + 1 - x, j
+    ).start()
+    for k in range(1, teams):
+        for copy in team_copies(k):
+            copy.start()
+    sall[j] = sact_ref[...]
+    gall[j] = gated_ref[...]
+    sdq[j] = columns(sd_ref, j)[...]
+    mwq[j] = columns(mw_ref, j)[...]
+    dq[j] = columns(d_ref, j)[...]
+
+    def forward(zb, d):
+        z_copy(zb, d).wait_recv()
+        to = z + 1 - 2 * d
+
+        @pl.when((to >= 0) & (to < lines))
+        def _():
+            z_copy(zb, d).start()
+
+        x_copy(zb).start()
+        c_copy(zb * 2 + x).start()
+
+    def activate(block):
+        rows = tok[block]
+        gate = jnp.dot(rows, g_ref[...], preferred_element_type=jnp.float32)
+        up = jnp.dot(rows, u_ref[...], preferred_element_type=jnp.float32)
+        act[block, j] = (gate / (1.0 + jnp.exp(-gate)) * up).astype(jnp.bfloat16)
+        for k in range(1, teams):
+            a_copy(block, k).start()
+
+    def finish(block):
+        for k in range(1, teams):
+            a_arrival(block, k).wait_recv()
+        total = jnp.dot(act[block, 0], dq[0], preferred_element_type=jnp.float32)
+        for q in range(1, teams):
+            total += jnp.dot(act[block, q], dq[q], preferred_element_type=jnp.float32)
+        return (total * wt_ref[block]).astype(jnp.bfloat16)
+
+    def xo_copy(zb):
+        return remote(
+            xout.at[zb], xin.at[zb], xo_send.at[zb], xo_recv.at[zb], z * 2 + 1 - x, j
+        )
+
+    def zo_copy(zb):
+        return remote(
+            zout.at[zb], zin.at[z], zo_send.at[zb], zo_recv.at[z], zb * 2 + x, j
+        )
+
+    def zo_arrival(zb):
+        return remote(
+            zout.at[zb], zin.at[zb], zo_send.at[zb], zo_recv.at[zb], zb * 2 + x, j
+        )
+
+    def valid(s, d, zb):
+        return (s >= 0) & (s < lines) & (zb >= 0) & (zb < lines) & ((s > 0) | (d == 0))
+
+    def step(t, carry):
+        def stage_one(d, carry):
+            s = t
+            zb = z + s * (2 * d - 1)
+
+            @pl.when(valid(s, d, zb) & (s > 0))
+            def _():
+                forward(zb, d)
+
+            return carry
+
+        lax.fori_loop(0, 2, stage_one, 0)
+
+        def stage_two(d, carry):
+            s = t - 1
+            zb = z + s * (2 * d - 1)
+
+            @pl.when(valid(s, d, zb))
+            def _():
+                x_arrival(zb).wait_recv()
+                c_copy(zb * 2 + 1 - x).start()
+
+                def column(n, carry):
+                    block = zb * 2 + lax.rem(x + n, 2)
+
+                    @pl.when(block != me)
+                    def _():
+                        c_arrival(block).wait_recv()
+
+                    activate(block)
+                    return carry
+
+                lax.fori_loop(0, 2, column, 0)
+
+            return carry
+
+        lax.fori_loop(0, 2, stage_two, 0)
+
+        @pl.when(t == 2)
+        def _():
+            for k in range(1, teams):
+                for copy in team_copies(k):
+                    copy.wait_recv()
+
+        def stage_three(d, carry):
+            s = t - 2
+            zb = z + s * (2 * d - 1)
+
+            @pl.when(valid(s, d, zb))
+            def _():
+                xout[zb] = finish(zb * 2 + 1 - x)
+                xo_copy(zb).start()
+                own[zb] = finish(zb * 2 + x)
+
+            return carry
+
+        lax.fori_loop(0, 2, stage_three, 0)
+
+        def stage_four(d, carry):
+            s = t - 3
+            zb = z + s * (2 * d - 1)
+
+            @pl.when(valid(s, d, zb))
+            def _():
+                xo_copy(zb).wait_recv()
+
+                @pl.when(s > 0)
+                def _():
+                    zout[zb] = (
+                        own[zb].astype(jnp.float32) + xin[zb].astype(jnp.float32)
+                    ).astype(jnp.bfloat16)
+                    zo_copy(zb).start()
+
+            return carry
+
+        lax.fori_loop(0, 2, stage_four, 0)
+        return carry
+
+    lax.fori_loop(1, lines + 3, step, 0)
+
+    def f_copies(k, source, rows):
+        p = lax.rem(j + k, teams)
+        return remote(
+            rows.at[source], rows.at[source],
+            f_send.at[0 if rows is fin else 1, k - 1], f_recv.at[0 if rows is fin else 1, k - 1],
+            me, p,
+        )
+
+    mixed = jnp.zeros(mfin.shape[1:], jnp.float32)
+    for q in range(teams):
+        mixed += (
+            jnp.dot(gall[q], mwq[q], preferred_element_type=jnp.float32)
+            .astype(jnp.bfloat16)
+            .astype(jnp.float32)
+        )
+    mfin[j] = mixed.astype(jnp.bfloat16)
+    for k in range(1, teams):
+        f_copies(k, j, mfin).start()
+
+    total = own[z].astype(jnp.float32) + xin[z].astype(jnp.float32)
+    for q in range(teams):
+        total += jnp.dot(sall[q], sdq[q], preferred_element_type=jnp.float32)
+    for k in range(1, lines):
+        source = lax.rem(z + k, lines)
+        zo_arrival(source).wait_recv()
+        total += zin[source].astype(jnp.float32)
+    fin[j] = total.astype(jnp.bfloat16)
+    for k in range(1, teams):
+        f_copies(k, j, fin).start()
+    for rows in (mfin, fin):
+        for k in range(1, teams):
+            f_copies(k, lax.rem(j + teams - k, teams), rows).wait_recv()
+    for q in range(teams):
+        mo_ref[:, q * quarter : (q + 1) * quarter] = mfin[q]
+        eo_ref[:, q * quarter : (q + 1) * quarter] = fin[q]
+
+    for k in range(1, teams):
+        f_copies(k, j, mfin).wait_send()
+        f_copies(k, j, fin).wait_send()
+        for copy in team_copies(k):
+            copy.wait_send()
+
+    def drain(zb, carry):
+        for way in range(2):
+            to = z + 1 - 2 * way
+            passing = (zb <= z) if way == 0 else (zb >= z)
+
+            @pl.when((to >= 0) & (to < lines) & passing)
+            def _():
+                z_copy(zb, way).wait_send()
+
+        x_copy(zb).wait_send()
+        xo_copy(zb).wait_send()
+
+        @pl.when(zb != z)
+        def _():
+            zo_copy(zb).wait_send()
+
+        def column(n, carry):
+            block = zb * 2 + n
+
+            @pl.when(block != me)
+            def _():
+                c_copy(block).wait_send()
+
+            for k in range(1, teams):
+                a_copy(block, k).wait_send()
+            return carry
+
+        lax.fori_loop(0, 2, column, 0)
+        return carry
+
+    lax.fori_loop(0, lines, drain, 0)
 
 
 def dense_experts(
+    gated_rows,
+    mix_weight,
     expert_input,
     norm_gain,
     route_ids,
@@ -90,38 +408,66 @@
     shared_down,
 ):
     ep_count = lax.axis_size("ep")
-    tp_count = lax.axis_size("tp")
-    tp_rank = lax.axis_index("tp")
-    ep_rank = lax.axis_index("ep")
-    tokens = expert_input.shape[0]
-    share = tokens // tp_count
+    teams = lax.axis_size("tp")
+    lines = ep_count // 2
+    tokens, width = expert_input.shape
+    quarter = width // teams
+    units = expert_gate.shape[2]
+    shared_units = shared_gate.shape[1]
+    length, channels = gated_rows.shape
     rows_wide = expert_input.astype(jnp.float32)
     normed = (
         rows_wide
         * lax.rsqrt(jnp.mean(rows_wide * rows_wide, axis=-1, keepdims=True) + epsilon)
         * norm_gain
     ).astype(jnp.bfloat16)
-    part = lax.dynamic_slice_in_dim(normed, tp_rank * share, share, 0)
-    everyone = lax.all_gather(part, ("ep", "tp"), axis=0, tiled=True)
     named = route_ids[:, :, None] == jnp.arange(ep_count, dtype=jnp.int32)[None, None, :]
     table = jnp.sum(jnp.where(named, route_weights[:, :, None], 0.0), axis=1).T
     table = lax.all_to_all(table, "ep", split_axis=0, concat_axis=1, tiled=True)
-    mine = table.reshape(ep_count * tokens)
-    gate_val = jnp.dot(everyone, expert_gate[0], preferred_element_type=jnp.float32)
-    up_val = jnp.dot(everyone, expert_up[0], preferred_element_type=jnp.float32)
-    hidden = (jax.nn.silu(gate_val) * up_val).astype(jnp.bfloat16)
-    partial_value = jnp.dot(hidden, expert_down[0], preferred_element_type=jnp.float32)
-    partial_value = (partial_value * mine[:, None]).astype(jnp.bfloat16)
-    routed = lax.psum_scatter(partial_value, ("ep", "tp"), scatter_dimension=0, tiled=True)
+    table = table.reshape(ep_count, tokens, 1)
     shared_gate_val = jnp.dot(normed, shared_gate, preferred_element_type=jnp.float32)
     shared_up_val = jnp.dot(normed, shared_up, preferred_element_type=jnp.float32)
     shared_act = (jax.nn.silu(shared_gate_val) * shared_up_val).astype(jnp.bfloat16)
-    shared = jnp.dot(shared_act, shared_down, preferred_element_type=jnp.float32)
-    shared = lax.psum_scatter(
-        shared.astype(jnp.bfloat16), "tp", scatter_dimension=0, tiled=True
-    )
-    piece = (routed.astype(jnp.float32) + shared.astype(jnp.float32)).astype(jnp.bfloat16)
-    return lax.all_gather(piece, "tp", axis=0, tiled=True)
+    low, dma = jnp.bfloat16, pltpu.SemaphoreType.DMA
+    vmem = pl.BlockSpec(memory_space=pltpu.VMEM)
+    expert_out, mixer_out = pl.pallas_call(
+        functools.partial(dense_kernel, lines, teams),
+        out_shape=(
+            jax.ShapeDtypeStruct((tokens, width), low),
+            jax.ShapeDtypeStruct((length, width), low),
+        ),
+        in_specs=[vmem] * 9,
+        out_specs=(vmem, vmem),
+        scratch_shapes=[
+            pltpu.VMEM((ep_count, tokens, width), low),
+            pltpu.VMEM((ep_count, teams, tokens, units), low),
+            pltpu.VMEM((teams, units, quarter), low),
+            pltpu.VMEM((teams, shared_units, quarter), low),
+            pltpu.VMEM((teams, channels, quarter), low),
+            pltpu.VMEM((teams, tokens, shared_units), low),
+            pltpu.VMEM((teams, length, channels), low),
+            pltpu.VMEM((lines, tokens, quarter), low),
+            pltpu.VMEM((lines, tokens, quarter), low),
+            pltpu.VMEM((lines, tokens, quarter), low),
+            pltpu.VMEM((lines, tokens, quarter), low),
+            pltpu.VMEM((lines, tokens, quarter), low),
+            pltpu.VMEM((teams, tokens, quarter), low),
+            pltpu.VMEM((teams, length, quarter), low),
+            dma((2, lines)), dma((lines,)), dma((lines,)), dma((lines,)),
+            dma((ep_count,)), dma((ep_count,)),
+            dma((ep_count, teams - 1)), dma((ep_count, teams - 1)),
+            dma((5, teams - 1)), dma((5, teams - 1)),
+            dma((lines,)), dma((lines,)), dma((lines,)), dma((lines,)),
+            dma((2, teams - 1)), dma((2, teams - 1)),
+        ],
+        compiler_params=pltpu.CompilerParams(
+            collective_id=0, has_side_effects=True, vmem_limit_bytes=56 * 1024 * 1024
+        ),
+    )(
+        normed, table, shared_act, gated_rows,
+        expert_gate[0], expert_up[0], expert_down[0], shared_down, mix_weight,
+    )
+    return mixer_out, expert_out
 
 
 def expert_half(
@@ -215,12 +561,12 @@
     ep_count, tp_count = lax.axis_size("ep"), lax.axis_size("tp")
     tokens, slots = expert_input.shape[0], route_ids.shape[1] * 2 * expert_input.shape[0]
     per_ep = tp_count * expert_gate.shape[2] // FF
-    dense = per_ep == 1 and slots // (ep_count * per_ep) >= tokens
-    mixer_partial = mixer_half(
+    even = ep_count % 2 == 0 and tp_count % 2 == 0
+    dense = even and per_ep == 1 and slots // (ep_count * per_ep) >= tokens
+    gated_rows = mixer_half(
         queries, key_vectors, values, out_gate, input_gate, forget_gate, mix_weight
     )
-    experts = dense_experts if dense else expert_half
-    expert_partial = experts(
+    experts = (
         expert_input,
         norm_gain,
         route_ids,
@@ -232,12 +578,14 @@
         shared_up,
         shared_down,
     )
+    if dense:
+        return dense_experts(gated_rows, mix_weight, *experts)
+    mixer_partial = jnp.dot(gated_rows, mix_weight, preferred_element_type=jnp.float32)
+    expert_partial = expert_half(*experts)
     mixer_piece = lax.psum_scatter(
         mixer_partial.astype(jnp.bfloat16), "tp", scatter_dimension=0, tiled=True
     )
     mixer_out = lax.all_gather(mixer_piece, "tp", axis=0, tiled=True)
-    if dense:
-        return (mixer_out, expert_partial)
     expert_piece = lax.psum_scatter(expert_partial, "tp", scatter_dimension=0, tiled=True).astype(
         jnp.bfloat16
     )

time: 315 us -> 199 us (0.63)
  waiting for transfers between devices: 225 us -> 13.8 us
  Pallas kernels: 0 us -> 127 us
  matrix products: 28.4 us -> 3.92 us
  blocking collectives: 23.5 us -> 16.9 us
    reduce_scatter x3 -> x0, waiting for transfers between devices: 144 us -> none  [the longest x1 120 us: dense_experts(): lax.psum_scatter(partial_value, ('ep', 'tp'), scatter_dimension=0, tiled=...]
    pallas_call x0 -> x1, Pallas kernels: none -> 127 us  [dense_experts(): pl.pallas_call(functools.partial(dense_kernel, lines, teams), out_shape=(...]
    all_gather x2 -> x0, waiting for transfers between devices: 80.4 us -> none  [the longest x1 68.5 us: dense_experts(): everyone = lax.all_gather(part, ('ep', 'tp'), axis=0, tiled=True)]
    dot_general x4 -> x2, matrix products: 24.7 us -> 1.91 us  [the longest x1 1.04 us: dense_experts(): jnp.dot(normed, shared_up, preferred_element_type=jnp.float32)]
    all_gather x1, waiting for transfers between devices: 0.01 us -> 13.7 us  [mixer_half(): lax.all_gather(jnp.concatenate([key_head, values], axis=1), 'ep', axis=0,...]
    all_gather x1 -> x0, blocking collectives: 7.48 us -> none  [shards(): mixer_out = lax.all_gather(mixer_piece, 'tp', axis=0, tiled=True)]
  transfers between devices with their start and end apart: 7 -> 2, of which waited for: 4 -> 1; matrix products, arithmetic and copies ran while one was open for 11% -> 6% of each run, Pallas kernels for 0% -> 0%
where the time goes in v2:
time: 199 us; the launch traced here: 198 us
  Pallas kernels  127 us (64%)
  blocking collectives  16.9 us (8%)
  between operations  14.2 us (7%)
  waiting for transfers between devices  13.8 us (7%)
  other arithmetic  8.64 us (4%)
  local copies, waits for them, and re-layouts  7.34 us (4%)
  starting transfers between devices  6.38 us (3%)
  matrix products  3.92 us (2%)
    pallas_call x1, Pallas kernels, dense_experts(): pl.pallas_call(functools.partial(dense_kernel, lines, teams), out_shape=(...  127 us
    all_gather x1, blocking collectives, mixer_half(): gates = lax.all_gather(gates, 'ep', axis=1, tiled=True)  16.9 us
    all_gather x1, waiting for transfers between devices, mixer_half(): lax.all_gather(jnp.concatenate([key_head, values], axis=1), 'ep', axis=0,...  13.7 us
    all_to_all x1, starting transfers between devices, dense_experts(): table = lax.all_to_all(table, 'ep', split_axis=0, concat_axis=1, tiled=True)  6.34 us
  transfers between devices with their start and end apart: 2, of which 1 were waited for; matrix products, arithmetic and copies ran while one was open for 6% of the time, Pallas kernels for 0%

profile of v2, /device:TPU:1, one launch (start us, length us, event | category | flops | bytes accessed | tf_op | source)
XLA Modules:
  0.0 198.1 jit_solution(16716012798594831372)
XLA Ops:
  7.2 0.0 copy-start
  7.2 0.0 copy-start.2
  7.2 0.0 copy-start.4
  7.2 0.8 select_reduce_fusion.1
  8.0 0.6 copy.27
  8.6 6.3 %all-to-all-start = ((f32[8,1,256]{2,1,0:T(1,128)}), f32[8,1,256]{2,1,0:T(1,128)S(1)}, u32[]{:S(2)}, u32[]{:S(2)}) async-start(f32[8,1,256]{2,1,0:T(1,128)} %copy.27), calls=%async_computation | async-start | bytes 16384 | tf_op jit(solution)/shard_map/all_to_all | solution.py:426
  15.0 0.0 all-gather.2.cloned.1.call-start
  15.0 0.8 constant_dynamic-slice_fusion.1
  15.9 1.5 pad_maximum_fusion
  17.4 0.0 all-gather.2.cloned.1.call-update
  17.4 0.8 select_reduce_fusion.4
  18.2 0.1 broadcast_bitcast_fusion.1
  18.3 16.9 %all_gather.7 = f32[2,1024]{1,0:T(2,128)S(1)} all-gather(f32[2,128]{1,0:T(2,128)S(1)} %pad_maximum_fusion.1), channel_id=1, replica_groups=mesh['ep'=8,'tp'=4] {'ep'}, dimensions={1}, use_global_device_ids=true | all-gather | bytes 9216 | tf_op jit(solution)/shard_map/all_gather | solution.py:44
  35.2 0.3 reduce_window_sum.13
  35.5 0.2 slice_reduce_fusion
  35.7 0.6 fusion.17
  36.3 0.1 select_reduce_fusion.2
  36.5 1.5 fusion
  38.0 0.1 broadcast_bitcast_fusion
  38.0 0.1 add_select_fusion
  38.1 1.9 select_reduce_fusion
  40.0 0.1 sub.45
  40.1 0.1 add.112
  40.1 0.1 fusion.12
  40.2 0.0 copy-done.2
  40.2 0.0 copy-done.4
  40.2 0.3 fusion.2.x_ref
  40.5 0.0 copy-done
  40.6 0.0 copy-start.1
  40.6 0.0 copy-start.6
  40.6 0.4 fusion.26
  41.0 1.0 copy-done.6
  42.0 1.0 fusion.5.sact_ref
  43.0 0.0 copy-done.1
  43.0 0.6 bitcast_maximum_fusion
  43.6 0.0 all-to-all-done
  43.7 1.4 reshape.333.wt_ref
  45.0 13.7 %all-gather.2.cloned.1.call-done = bf16[1024,512]{1,0:T(8,128)(2,1)} async-done(((bf16[128,512]{1,0:T(8,128)(2,1)}), bf16[1024,512]{1,0:T(8,128)(2,1)}) %all-gather.2.cloned.1.call-update) | async-done | bytes 1048592 | tf_op jit(solution)/shard_map/all_gather | solution.py:34
  58.8 0.1 and.56
  58.9 0.0 copy-done.7
  58.9 0.0 copy-start.5
  58.9 0.0 copy-start.8
  58.9 1.6 fusion.25
  60.5 0.9 fusion.6.gated_ref
  61.4 126.9 %shard_map.176 = (bf16[256,2048]{1,0:T(8,128)(2,1)}, bf16[128,2048]{1,0:T(8,128)(2,1)}) custom-call(bf16[256,2048]{1,0:T(8,128)(2,1)} %copy-done.1, f32[8,256,1]{2,1,0:T(8,128)} %reshape.333.wt_ref, bf16[256,128]{1,0:T(8,128)(2,1)} %fusion.5.sact_ref, bf16[128,256]{1,0:T(8,128)(2,1)} %fusion.6.gated_ref, bf16[2048,256]{1,0:T(8,128)(2,1)} %bitcast.63, ...), custom_call_target="tpu_custom_call" | custom-call | tf_op jit(solution)/shard_map/pallas_call | solution.py:433
  188.3 2.0 copy.33
  190.3 0.0 copy-done.3
  190.3 1.0 copy.34
  (14 shorter events, 0.1 us)
Async XLA Ops:
  7.2 33.4 %copy-start = (bf16[2048,128]{1,0:T(8,128)(2,1)S(1)}, bf16[2048,128]{1,0:T(8,128)(2,1)}, u32[]{:S(2)}) copy-start(bf16[2048,128]{1,0:T(8,128)(2,1)} %param.31) | copy-start | bytes 1572868
  7.2 33.0 %copy-start.2 = (bf16[256,2048]{1,0:T(8,128)(2,1)S(1)}, bf16[256,2048]{1,0:T(8,128)(2,1)}, u32[]{:S(2)}) copy-start(bf16[256,2048]{1,0:T(8,128)(2,1)} %param.24) | copy-start | bytes 3145732
  7.2 33.0 %copy-start.4 = (f32[2048]{0:T(1024)S(1)}, f32[2048]{0:T(1024)}, u32[]{:S(2)}) copy-start(f32[2048]{0:T(1024)} %param.25) | copy-start | bytes 24580
  8.6 35.0 %all-to-all-start = ((f32[8,1,256]{2,1,0:T(1,128)}), f32[8,1,256]{2,1,0:T(1,128)S(1)}, u32[]{:S(2)}, u32[]{:S(2)}) async-start(f32[8,1,256]{2,1,0:T(1,128)} %copy.27), calls=%async_computation | async-start | bytes 16384 | tf_op jit(solution)/shard_map/all_to_all | solution.py:426
  15.0 43.8 %all-gather.2.cloned.1.call-start = ((), (), s32[]{:S(2)}) async-start(), calls=%async_computation.1 | async-start | bytes 1179648 | tf_op jit(solution)/shard_map/all_gather | solution.py:34
  40.6 2.5 %copy-start.1 = (bf16[256,2048]{1,0:T(8,128)(2,1)}, bf16[256,2048]{1,0:T(8,128)(2,1)S(1)}, u32[]{:S(2)}) copy-start(bf16[256,2048]{1,0:T(8,128)(2,1)S(1)} %fusion.2.x_ref) | copy-start | bytes 3145732
  40.6 1.4 copy-start.6
  43.0 15.8 %copy-start.7 = (bf16[128,512]{1,0:T(8,128)(2,1)S(1)}, bf16[128,512]{1,0:T(8,128)(2,1)}, u32[]{:S(2)}) copy-start(bf16[128,512]{1,0:T(8,128)(2,1)} %param.17) | copy-start | bytes 393220
  58.9 1.6 copy-start.5
  58.9 1.6 copy-start.8
  188.3 2.0 %copy-start.3 = (bf16[256,2048]{1,0:T(8,128)(2,1)S(1)}, bf16[256,2048]{1,0:T(8,128)(2,1)}, u32[]{:S(2)}) copy-start(bf16[256,2048]{1,0:T(8,128)(2,1)} %get-tuple-element.19) | copy-start | bytes 3145732
Sparse Core Ops, SparseCore 0:
  18.5 40.2 all-gather.1

commit v3 on v2

--- a/solution.py
+++ b/solution.py
@@ -19,21 +19,13 @@
 den_floor = 4.0
 
 
-def mixer_half(queries, key_vectors, values, out_gate, input_gate, forget_gate, mix_weight):
+def mixer_local(queries, key_vectors, values, input_gate, forget_gate):
     tp_count = lax.axis_size("tp")
     tp_rank = lax.axis_index("tp")
-    ep_count = lax.axis_size("ep")
-    ep_rank = lax.axis_index("ep")
-    length = queries.shape[0]
-    channels = values.shape[1]
-    factor = KEY_DIM ** (-0.5)
     head_index = tp_rank // (tp_count // MEMORY_HEADS)
     offset = head_index * KEY_DIM
     query_head = lax.dynamic_slice_in_dim(queries, offset, KEY_DIM, 1)
     key_head = lax.dynamic_slice_in_dim(key_vectors, offset, KEY_DIM, 1)
-    both = lax.all_gather(jnp.concatenate([key_head, values], axis=1), "ep", axis=0, tiled=True)
-    keys_all = both[:, :KEY_DIM]
-    values_all = both[:, KEY_DIM:]
     select = jnp.arange(MEMORY_HEADS, dtype=jnp.int32)[None, :] == head_index
     gates = jnp.stack(
         [
@@ -41,7 +33,16 @@
             jax.nn.log_sigmoid(jnp.sum(jnp.where(select, forget_gate, 0.0), axis=1)),
         ]
     )
-    gates = lax.all_gather(gates, "ep", axis=1, tiled=True)
+    return query_head, jnp.concatenate([key_head, values], axis=1), gates
+
+
+def mixer_rows(query_head, both, gates, out_gate):
+    ep_count = lax.axis_size("ep")
+    ep_rank = lax.axis_index("ep")
+    length = query_head.shape[0]
+    factor = KEY_DIM ** (-0.5)
+    keys_all = both[:, :KEY_DIM]
+    values_all = both[:, KEY_DIM:]
     total = ep_count * length
     blocks = total // BLOCK
     mine = length // BLOCK
@@ -82,16 +83,17 @@
 
 
 def dense_kernel(
-    lines, teams, x_ref, wt_ref, sact_ref, gated_ref, g_ref, u_ref, d_ref, sd_ref, mw_ref,
-    eo_ref, mo_ref,
-    tok, act, dq, sdq, mwq, sall, gall, xout, xin, own, zout, zin, fin, mfin,
+    lines, teams, x_ref, side_ref, kv_ref, sact_ref, g_ref, u_ref, d_ref, sd_ref, mw_ref,
+    eo_ref, kvo_ref, so_ref, mwo_ref,
+    tok, act, dq, sdq, mwq, sall, kvb, sideb, xout, xin, own, zout, zin, fin,
     z_send, z_recv, x_send, x_recv, c_send, c_recv, a_send, a_recv,
-    w_send, w_recv, xo_send, xo_recv, zo_send, zo_recv, f_send, f_recv,
+    k_send, k_recv, kx_send, kx_recv, w_send, w_recv, xo_send, xo_recv, zo_send, zo_recv, f_send, f_recv,
 ):
     me = lax.axis_index("ep")
     j = lax.axis_index("tp")
     z, x = me // 2, me % 2
-    half_rows = x_ref.shape[0] // 2
+    tokens = x_ref.shape[0]
+    half_rows = tokens // 2
     core = j % 2
     buddy = j + 1 - 2 * core
     quarter = fin.shape[2]
@@ -126,7 +128,6 @@
         pairs = (
             (sact_ref, sall.at[j]),
             (columns(sd_ref, p), sdq.at[j]),
-            (gated_ref, gall.at[j]),
             (columns(mw_ref, p), mwq.at[j]),
             (columns(d_ref, p), dq.at[j]),
         )
@@ -170,7 +171,24 @@
             a_send.at[block, k - 1], a_recv.at[block, k - 1], me, p,
         )
 
+    extras = (sideb, kvb)
+
+    def k_copy(n, zb, way):
+        to = z + 1 - 2 * way
+        ref = extras[n].at[zb * 2 + x]
+        return remote(ref, ref, k_send.at[n, way, zb], k_recv.at[n, zb], to * 2 + x, j)
+
+    def kx_copy(n, zb):
+        ref = extras[n].at[zb * 2 + x]
+        return remote(ref, ref, kx_send.at[n, zb], kx_recv.at[n, zb], z * 2 + 1 - x, j)
+
+    def kx_arrival(n, zb):
+        ref = extras[n].at[zb * 2 + 1 - x]
+        return remote(ref, ref, kx_send.at[n, zb], kx_recv.at[n, zb], z * 2 + 1 - x, j)
+
     tok[me] = x_ref[...]
+    sideb[me] = side_ref[...]
+    kvb[me] = kv_ref[...]
     for way in range(2):
         to = z + 1 - 2 * way
 
@@ -180,15 +198,22 @@
                 x_ref.at[mine_rows], tok.at[me, mine_rows],
                 z_send.at[way, z], z_recv.at[z], to * 2 + x, j,
             ).start()
+            for n, ref in enumerate((side_ref, kv_ref)):
+                remote(
+                    ref, extras[n].at[me], k_send.at[n, way, z], k_recv.at[n, z], to * 2 + x, j
+                ).start()
 
     remote(
         x_ref.at[mine_rows], tok.at[me, mine_rows], x_send.at[z], x_recv.at[z], z * 2 + 1 - x, j
     ).start()
+    for n, ref in enumerate((side_ref, kv_ref)):
+        remote(
+            ref, extras[n].at[me], kx_send.at[n, z], kx_recv.at[n, z], z * 2 + 1 - x, j
+        ).start()
     for k in range(1, teams):
         for copy in team_copies(k):
             copy.start()
     sall[j] = sact_ref[...]
-    gall[j] = gated_ref[...]
     sdq[j] = columns(sd_ref, j)[...]
     mwq[j] = columns(mw_ref, j)[...]
     dq[j] = columns(d_ref, j)[...]
@@ -203,6 +228,14 @@
 
         x_copy(zb).start()
         c_copy(zb * 2 + x).start()
+        for n in range(2):
+            k_copy(n, zb, d).wait_recv()
+
+            @pl.when((to >= 0) & (to < lines))
+            def _():
+                k_copy(n, zb, d).start()
+
+            kx_copy(n, zb).start()
 
     def activate(block):
         rows = tok[block]
@@ -218,7 +251,11 @@
         total = jnp.dot(act[block, 0], dq[0], preferred_element_type=jnp.float32)
         for q in range(1, teams):
             total += jnp.dot(act[block, q], dq[q], preferred_element_type=jnp.float32)
-        return (total * wt_ref[block]).astype(jnp.bfloat16)
+        weight = sideb[block, pl.ds(me, 1), :tokens]
+        row = lax.broadcasted_iota(jnp.int32, (tokens, tokens), 0)
+        lane = lax.broadcasted_iota(jnp.int32, (tokens, tokens), 1)
+        weight = jnp.sum(jnp.where(row == lane, weight, 0.0), axis=1, keepdims=True)
+        return (total * weight).astype(jnp.bfloat16)
 
     def xo_copy(zb):
         return remote(
@@ -259,6 +296,8 @@
             def _():
                 x_arrival(zb).wait_recv()
                 c_copy(zb * 2 + 1 - x).start()
+                for n in range(2):
+                    kx_arrival(n, zb).wait_recv()
 
                 def column(n, carry):
                     block = zb * 2 + lax.rem(x + n, 2)
@@ -322,20 +361,9 @@
         p = lax.rem(j + k, teams)
         return remote(
             rows.at[source], rows.at[source],
-            f_send.at[0 if rows is fin else 1, k - 1], f_recv.at[0 if rows is fin else 1, k - 1],
+            f_send.at[k - 1], f_recv.at[k - 1],
             me, p,
         )
-
-    mixed = jnp.zeros(mfin.shape[1:], jnp.float32)
-    for q in range(teams):
-        mixed += (
-            jnp.dot(gall[q], mwq[q], preferred_element_type=jnp.float32)
-            .astype(jnp.bfloat16)
-            .astype(jnp.float32)
-        )
-    mfin[j] = mixed.astype(jnp.bfloat16)
-    for k in range(1, teams):
-        f_copies(k, j, mfin).start()
 
     total = own[z].astype(jnp.float32) + xin[z].astype(jnp.float32)
     for q in range(teams):
@@ -347,15 +375,15 @@
     fin[j] = total.astype(jnp.bfloat16)
     for k in range(1, teams):
         f_copies(k, j, fin).start()
-    for rows in (mfin, fin):
-        for k in range(1, teams):
-            f_copies(k, lax.rem(j + teams - k, teams), rows).wait_recv()
+    kvo_ref[...] = kvb[...]
+    so_ref[...] = sideb[...]
+    mwo_ref[...] = mwq[...]
+    for k in range(1, teams):
+        f_copies(k, lax.rem(j + teams - k, teams), fin).wait_recv()
     for q in range(teams):
-        mo_ref[:, q * quarter : (q + 1) * quarter] = mfin[q]
         eo_ref[:, q * quarter : (q + 1) * quarter] = fin[q]
 
     for k in range(1, teams):
-        f_copies(k, j, mfin).wait_send()
         f_copies(k, j, fin).wait_send()
         for copy in team_copies(k):
             copy.wait_send()
@@ -368,8 +396,12 @@
             @pl.when((to >= 0) & (to < lines) & passing)
             def _():
                 z_copy(zb, way).wait_send()
+                for n in range(2):
+                    k_copy(n, zb, way).wait_send()
 
         x_copy(zb).wait_send()
+        for n in range(2):
+            kx_copy(n, zb).wait_send()
         xo_copy(zb).wait_send()
 
         @pl.when(zb != z)
@@ -393,8 +425,56 @@
     lax.fori_loop(0, lines, drain, 0)
 
 
+def project_kernel(teams, gated_ref, mwq_ref, mo_ref, gall, mfin, g_send, g_recv, f_send, f_recv):
+    me = lax.axis_index("ep")
+    j = lax.axis_index("tp")
+    quarter = mfin.shape[2]
+
+    def copy(ref, source, send, recv, k):
+        return pltpu.make_async_remote_copy(
+            src_ref=ref, dst_ref=source, send_sem=send.at[k - 1], recv_sem=recv.at[k - 1],
+            device_id={"ep": me, "tp": lax.rem(j + k, teams)},
+            device_id_type=pl.DeviceIdType.MESH,
+        )
+
+    barrier = pltpu.get_barrier_semaphore()
+    for k in range(1, teams):
+        pl.semaphore_signal(
+            barrier, inc=1, device_id={"ep": me, "tp": lax.rem(j + k, teams)},
+            device_id_type=pl.DeviceIdType.MESH,
+        )
+    pl.semaphore_wait(barrier, teams - 1)
+    for k in range(1, teams):
+        copy(gated_ref, gall.at[j], g_send, g_recv, k).start()
+    gall[j] = gated_ref[...]
+    for k in range(1, teams):
+        source = lax.rem(j + teams - k, teams)
+        copy(gated_ref, gall.at[source], g_send, g_recv, k).wait_recv()
+    mixed = jnp.zeros(mfin.shape[1:], jnp.float32)
+    for q in range(teams):
+        mixed += (
+            jnp.dot(gall[q], mwq_ref[q], preferred_element_type=jnp.float32)
+            .astype(jnp.bfloat16)
+            .astype(jnp.float32)
+        )
+    mfin[j] = mixed.astype(jnp.bfloat16)
+    for k in range(1, teams):
+        copy(mfin.at[j], mfin.at[j], f_send, f_recv, k).start()
+    for k in range(1, teams):
+        source = lax.rem(j + teams - k, teams)
+        copy(mfin.at[source], mfin.at[source], f_send, f_recv, k).wait_recv()
+    for q in range(teams):
+        mo_ref[:, q * quarter : (q + 1) * quarter] = mfin[q]
+    for k in range(1, teams):
+        copy(gated_ref, gall.at[j], g_send, g_recv, k).wait_send()
+        copy(mfin.at[j], mfin.at[j], f_send, f_recv, k).wait_send()
+
+
 def dense_experts(
-    gated_rows,
+    query_head,
+    both,
+    gates,
+    out_gate,
     mix_weight,
     expert_input,
     norm_gain,
@@ -414,7 +494,7 @@
     quarter = width // teams
     units = expert_gate.shape[2]
     shared_units = shared_gate.shape[1]
-    length, channels = gated_rows.shape
+    length, channels = both.shape[0], mix_weight.shape[0]
     rows_wide = expert_input.astype(jnp.float32)
     normed = (
         rows_wide
@@ -423,21 +503,28 @@
     ).astype(jnp.bfloat16)
     named = route_ids[:, :, None] == jnp.arange(ep_count, dtype=jnp.int32)[None, None, :]
     table = jnp.sum(jnp.where(named, route_weights[:, :, None], 0.0), axis=1).T
-    table = lax.all_to_all(table, "ep", split_axis=0, concat_axis=1, tiled=True)
-    table = table.reshape(ep_count, tokens, 1)
+    lanes = max(tokens, length)
+    side = jnp.concatenate(
+        [
+            jnp.pad(table, ((0, 0), (0, lanes - tokens))),
+            jnp.pad(gates, ((0, -(ep_count + 2) % 8), (0, lanes - length))),
+        ]
+    )
     shared_gate_val = jnp.dot(normed, shared_gate, preferred_element_type=jnp.float32)
     shared_up_val = jnp.dot(normed, shared_up, preferred_element_type=jnp.float32)
     shared_act = (jax.nn.silu(shared_gate_val) * shared_up_val).astype(jnp.bfloat16)
     low, dma = jnp.bfloat16, pltpu.SemaphoreType.DMA
     vmem = pl.BlockSpec(memory_space=pltpu.VMEM)
-    expert_out, mixer_out = pl.pallas_call(
+    expert_out, both_all, side_all, mix_all = pl.pallas_call(
         functools.partial(dense_kernel, lines, teams),
         out_shape=(
             jax.ShapeDtypeStruct((tokens, width), low),
-            jax.ShapeDtypeStruct((length, width), low),
+            jax.ShapeDtypeStruct((ep_count, *both.shape), low),
+            jax.ShapeDtypeStruct((ep_count, *side.shape), jnp.float32),
+            jax.ShapeDtypeStruct((teams, channels, quarter), low),
         ),
         in_specs=[vmem] * 9,
-        out_specs=(vmem, vmem),
+        out_specs=(vmem, vmem, vmem, vmem),
         scratch_shapes=[
             pltpu.VMEM((ep_count, tokens, width), low),
             pltpu.VMEM((ep_count, teams, tokens, units), low),
@@ -445,28 +532,48 @@
             pltpu.VMEM((teams, shared_units, quarter), low),
             pltpu.VMEM((teams, channels, quarter), low),
             pltpu.VMEM((teams, tokens, shared_units), low),
-            pltpu.VMEM((teams, length, channels), low),
+            pltpu.VMEM((ep_count, *both.shape), low),
+            pltpu.VMEM((ep_count, *side.shape), jnp.float32),
             pltpu.VMEM((lines, tokens, quarter), low),
             pltpu.VMEM((lines, tokens, quarter), low),
             pltpu.VMEM((lines, tokens, quarter), low),
             pltpu.VMEM((lines, tokens, quarter), low),
             pltpu.VMEM((lines, tokens, quarter), low),
             pltpu.VMEM((teams, tokens, quarter), low),
-            pltpu.VMEM((teams, length, quarter), low),
             dma((2, lines)), dma((lines,)), dma((lines,)), dma((lines,)),
             dma((ep_count,)), dma((ep_count,)),
             dma((ep_count, teams - 1)), dma((ep_count, teams - 1)),
-            dma((5, teams - 1)), dma((5, teams - 1)),
+            dma((2, 2, lines)), dma((2, lines)), dma((2, lines)), dma((2, lines)),
+            dma((4, teams - 1)), dma((4, teams - 1)),
             dma((lines,)), dma((lines,)), dma((lines,)), dma((lines,)),
-            dma((2, teams - 1)), dma((2, teams - 1)),
+            dma((teams - 1,)), dma((teams - 1,)),
         ],
         compiler_params=pltpu.CompilerParams(
             collective_id=0, has_side_effects=True, vmem_limit_bytes=56 * 1024 * 1024
         ),
     )(
-        normed, table, shared_act, gated_rows,
+        normed, side, both, shared_act,
         expert_gate[0], expert_up[0], expert_down[0], shared_down, mix_weight,
     )
+    gates_all = side_all[:, ep_count : ep_count + 2, :length].transpose(1, 0, 2)
+    gated_rows = mixer_rows(
+        query_head,
+        both_all.reshape(ep_count * length, both.shape[1]),
+        gates_all.reshape(2, ep_count * length),
+        out_gate,
+    )
+    mixer_out = pl.pallas_call(
+        functools.partial(project_kernel, teams),
+        out_shape=jax.ShapeDtypeStruct((length, width), low),
+        in_specs=[vmem] * 2,
+        out_specs=vmem,
+        scratch_shapes=[
+            pltpu.VMEM((teams, length, channels), low),
+            pltpu.VMEM((teams, length, quarter), low),
+            dma((teams - 1,)), dma((teams - 1,)), dma((teams - 1,)), dma((teams - 1,)),
+        ],
+        compiler_params=pltpu.CompilerParams(collective_id=1, has_side_effects=True),
+    )(gated_rows, mix_all)
     return mixer_out, expert_out
 
 
@@ -563,8 +670,8 @@
     per_ep = tp_count * expert_gate.shape[2] // FF
     even = ep_count % 2 == 0 and tp_count % 2 == 0
     dense = even and per_ep == 1 and slots // (ep_count * per_ep) >= tokens
-    gated_rows = mixer_half(
-        queries, key_vectors, values, out_gate, input_gate, forget_gate, mix_weight
+    query_head, both, gates = mixer_local(
+        queries, key_vectors, values, input_gate, forget_gate
     )
     experts = (
         expert_input,
@@ -579,7 +686,10 @@
         shared_down,
     )
     if dense:
-        return dense_experts(gated_rows, mix_weight, *experts)
+        return dense_experts(query_head, both, gates, out_gate, mix_weight, *experts)
+    both = lax.all_gather(both, "ep", axis=0, tiled=True)
+    gates = lax.all_gather(gates, "ep", axis=1, tiled=True)
+    gated_rows = mixer_rows(query_head, both, gates, out_gate)
     mixer_partial = jnp.dot(gated_rows, mix_weight, preferred_element_type=jnp.float32)
     expert_partial = expert_half(*experts)
     mixer_piece = lax.psum_scatter(

time: 199 us -> 161 us (0.81)
  blocking collectives: 16.9 us -> 0 us
  Pallas kernels: 127 us -> 141 us
  waiting for transfers between devices: 13.8 us -> 0 us
  between operations: 14.2 us -> 0.83 us
  starting transfers between devices: 6.38 us -> 0 us
    all_gather x1 -> x0, blocking collectives: 16.9 us -> none  [mixer_half(): gates = lax.all_gather(gates, 'ep', axis=1, tiled=True)]
    pallas_call x0 -> x1, Pallas kernels: none -> 16 us  [dense_experts(): pl.pallas_call(functools.partial(project_kernel, teams), out_shape=jax.Sh...]
    all_gather x1 -> x0, waiting for transfers between devices: 13.7 us -> none  [mixer_half(): lax.all_gather(jnp.concatenate([key_head, values], axis=1), 'ep', axis=0,...]
    all_to_all x1 -> x0, starting transfers between devices: 6.34 us -> none  [dense_experts(): table = lax.all_to_all(table, 'ep', split_axis=0, concat_axis=1, tiled=True)]
    pallas_call x1, Pallas kernels: 127 us -> 125 us  [dense_experts(): pl.pallas_call(functools.partial(dense_kernel, lines, teams), out_shape=(...]
  transfers between devices with their start and end apart: 2 -> 0, of which waited for: 1 -> 0; matrix products, arithmetic and copies ran while one was open for 6% -> 0% of each run, Pallas kernels for 0% -> 0%
where the time goes in v3:
time: 161 us
  Pallas kernels  141 us (88%)
  other arithmetic  9.1 us (6%)
  local copies, waits for them, and re-layouts  6.01 us (4%)
  matrix products  3.93 us (2%)
    pallas_call x1, Pallas kernels, dense_experts(): pl.pallas_call(functools.partial(dense_kernel, lines, teams), out_shape=(...  125 us
    pallas_call x1, Pallas kernels, dense_experts(): pl.pallas_call(functools.partial(project_kernel, teams), out_shape=jax.Sh...  16 us
    unnamed x20, local copies, waits for them, and re-layouts  3.89 us

profile of v3, /device:TPU:1, one launch (start us, length us, event | category | flops | bytes accessed | tf_op | source)
XLA Modules:
  0.0 160.5 jit_solution(11561518709051041158)
XLA Ops:
  0.6 0.0 copy-start
  0.6 0.0 copy-start.2
  0.7 0.0 copy-start.4
  0.7 1.0 constant_dynamic-slice_fusion.1
  1.6 1.5 pad_maximum_fusion.kv_ref
  3.2 0.8 select_reduce_fusion.4
  4.0 0.7 select_reduce_fusion.1
  4.7 0.6 pad_maximum_fusion.1.side_ref
  5.3 1.5 fusion
  6.8 0.0 copy-done.2
  6.8 0.0 copy-done.4
  6.8 0.3 fusion.2.x_ref
  7.1 0.0 copy-done
  7.1 0.0 copy-start.1
  7.2 0.0 copy-start.6
  7.2 0.4 fusion.22
  7.6 1.0 copy-done.6
  8.6 1.0 fusion.5.sact_ref
  9.6 0.0 copy-done.1
  9.6 0.0 copy-start.7
  9.6 124.6 %shard_map.176 = (bf16[256,2048]{1,0:T(8,128)(2,1)}, bf16[8,128,512]{2,1,0:T(8,128)(2,1)}, f32[8,16,256]{2,1,0:T(8,128)}, bf16[4,256,512]{2,1,0:T(8,128)(2,1)}) custom-call(bf16[256,2048]{1,0:T(8,128)(2,1)} %copy-done.1, f32[16,256]{1,0:T(8,128)} %pad_maximum_fusion.1.side_ref, bf16[128,512]{1,0:T(8,128)(2,1)} %pad_maximum_fusion.kv_ref, ...), custom_call_target="tpu_custom_call" | custom-call | tf_op jit(solution)/shard_map/pallas_call | solution.py:518
  134.2 0.8 slice_bitcast_fusion
  135.0 0.3 reduce_window_sum.13
  135.3 0.2 slice_reduce_fusion
  135.5 0.1 select_reduce_fusion.2
  135.6 0.1 broadcast_select_fusion
  135.7 1.9 %select_reduce_fusion = f32[128]{0:T(128)S(1)} fusion(f32[8,128]{1,0:T(8,128)S(1)} %bitcast.56, f32[128]{0:T(128)S(1)} %fusion.20, pred[8]{0:T(512)(128)(4,1)S(1)} %get-tuple-element.15, pred[128,128]{1,0:T(8,128)(4,1)S(1)} %iota_compare_fusion, pred[8]{0:T(512)(128)(4,1)S(1)} %get-tuple-element.14), kind=kLoop, calls=%fused_computation.14 | loop fusion | flops 655232 | bytes 21520 | tf_op jit(solution)/shard_map/reduce_max | solution.py:70
  137.6 0.6 fusion.14
  138.2 0.7 bitcast_maximum_fusion
  138.9 0.1 broadcast_bitcast_fusion
  138.9 0.1 broadcast_bitcast_fusion.1
  139.0 0.1 and.56
  139.1 0.0 copy-done.7
  139.1 0.0 copy-start.5
  139.1 0.0 copy-start.8
  139.1 1.6 fusion.21
  140.7 0.0 copy-done.5
  140.7 0.0 copy-done.8
  140.7 0.9 fusion.6.gated_ref
  141.6 0.0 copy-start.3
  141.6 16.0 %shard_map.177 = bf16[128,2048]{1,0:T(8,128)(2,1)} custom-call(bf16[128,256]{1,0:T(8,128)(2,1)} %fusion.6.gated_ref, bf16[4,256,512]{2,1,0:T(8,128)(2,1)} %get-tuple-element.8.mwq_ref), custom_call_target="tpu_custom_call" | custom-call | tf_op jit(solution)/shard_map/pallas_call | solution.py:565
  157.7 1.9 %copy.27 = bf16[128,2048]{1,0:T(8,128)(2,1)} copy(bf16[128,2048]{1,0:T(8,128)(2,1)} %shard_map.177) | data formatting | bytes 1048576
  159.5 0.0 copy-done.3
  159.5 1.0 copy.28
  (9 shorter events, 0.1 us)
Async XLA Ops:
  0.6 6.5 %copy-start = (bf16[2048,128]{1,0:T(8,128)(2,1)S(1)}, bf16[2048,128]{1,0:T(8,128)(2,1)}, u32[]{:S(2)}) copy-start(bf16[2048,128]{1,0:T(8,128)(2,1)} %param.31) | copy-start | bytes 1572868
  0.6 6.2 %copy-start.2 = (bf16[256,2048]{1,0:T(8,128)(2,1)S(1)}, bf16[256,2048]{1,0:T(8,128)(2,1)}, u32[]{:S(2)}) copy-start(bf16[256,2048]{1,0:T(8,128)(2,1)} %param.24) | copy-start | bytes 3145732
  0.7 6.2 %copy-start.4 = (f32[2048]{0:T(1024)S(1)}, f32[2048]{0:T(1024)}, u32[]{:S(2)}) copy-start(f32[2048]{0:T(1024)} %param.25) | copy-start | bytes 24580
  7.1 2.5 %copy-start.1 = (bf16[256,2048]{1,0:T(8,128)(2,1)}, bf16[256,2048]{1,0:T(8,128)(2,1)S(1)}, u32[]{:S(2)}) copy-start(bf16[256,2048]{1,0:T(8,128)(2,1)S(1)} %fusion.2.x_ref) | copy-start | bytes 3145732
  7.2 1.4 copy-start.6
  9.6 129.4 %copy-start.7 = (bf16[128,512]{1,0:T(8,128)(2,1)S(1)}, bf16[128,512]{1,0:T(8,128)(2,1)}, u32[]{:S(2)}) copy-start(bf16[128,512]{1,0:T(8,128)(2,1)} %param.17) | copy-start | bytes 393220
  139.1 1.6 %copy-start.5 = (bf16[8,128,512]{2,1,0:T(8,128)(2,1)S(1)}, bf16[8,128,512]{2,1,0:T(8,128)(2,1)}, u32[]{:S(2)}) copy-start(bf16[8,128,512]{2,1,0:T(8,128)(2,1)} %get-tuple-element.6) | copy-start | bytes 3145732
  139.1 1.6 %copy-start.8 = (bf16[128,256]{1,0:T(8,128)(2,1)S(1)}, bf16[128,256]{1,0:T(8,128)(2,1)}, u32[]{:S(2)}) copy-start(bf16[128,256]{1,0:T(8,128)(2,1)} %param.20) | copy-start | bytes 196612
  141.6 17.9 %copy-start.3 = (bf16[256,2048]{1,0:T(8,128)(2,1)S(1)}, bf16[256,2048]{1,0:T(8,128)(2,1)}, u32[]{:S(2)}) copy-start(bf16[256,2048]{1,0:T(8,128)(2,1)} %get-tuple-element.21) | copy-start | bytes 3145732

commit v4 on v3

--- a/solution.py
+++ b/solution.py
@@ -164,13 +164,6 @@
             a_send.at[block, k - 1], a_recv.at[block, k - 1], me, p,
         )
 
-    def a_arrival(block, k):
-        p = lax.rem(j + teams - k, teams)
-        return remote(
-            act.at[block, p], act.at[block, p],
-            a_send.at[block, k - 1], a_recv.at[block, k - 1], me, p,
-        )
-
     extras = (sideb, kvb)
 
     def k_copy(n, zb, way):
@@ -242,12 +235,22 @@
         gate = jnp.dot(rows, g_ref[...], preferred_element_type=jnp.float32)
         up = jnp.dot(rows, u_ref[...], preferred_element_type=jnp.float32)
         act[block, j] = (gate / (1.0 + jnp.exp(-gate)) * up).astype(jnp.bfloat16)
-        for k in range(1, teams):
-            a_copy(block, k).start()
+        for e in range(1, teams // 2):
+            a_move(block, j, e - 1, lax.rem(j + 2 * e, teams)).start()
+        a_move(block, j, teams // 2 - 1, buddy).start()
+
+    def a_move(block, source, slot, to):
+        ref = act.at[block, source]
+        return remote(ref, ref, a_send.at[block, slot], a_recv.at[block, slot], me, to)
 
     def finish(block):
-        for k in range(1, teams):
-            a_arrival(block, k).wait_recv()
+        for e in range(1, teams // 2):
+            source = lax.rem(j + teams - 2 * e, teams)
+            a_move(block, source, e - 1, source).wait_recv()
+            a_move(block, source, teams // 2 - 1 + e, buddy).start()
+        for e in range(teams // 2):
+            source = lax.rem(buddy + teams - 2 * e, teams)
+            a_move(block, source, teams // 2 - 1 + e, buddy).wait_recv()
         total = jnp.dot(act[block, 0], dq[0], preferred_element_type=jnp.float32)
         for q in range(1, teams):
             total += jnp.dot(act[block, q], dq[q], preferred_element_type=jnp.float32)

time: 161 us -> 158 us (0.981); the launches traced: 161 us -> 155 us
  Pallas kernels: 141 us -> 135 us
    pallas_call x1, Pallas kernels: 125 us -> 120 us  [dense_experts(): pl.pallas_call(functools.partial(dense_kernel, lines, teams), out_shape=(...]
where the time goes in v4:
time: 158 us; the launch traced here: 155 us
  Pallas kernels  135 us (85%)
  other arithmetic  9.1 us (6%)
  local copies, waits for them, and re-layouts  6.01 us (4%)
  matrix products  3.93 us (2%)
    pallas_call x1, Pallas kernels, dense_experts(): pl.pallas_call(functools.partial(dense_kernel, lines, teams), out_shape=(...  120 us
    pallas_call x1, Pallas kernels, dense_experts(): pl.pallas_call(functools.partial(project_kernel, teams), out_shape=jax.Sh...  14.9 us
    unnamed x20, local copies, waits for them, and re-layouts  3.89 us

profile of v4, /device:TPU:1, one launch (start us, length us, event | category | flops | bytes accessed | tf_op | source)
XLA Modules:
  0.0 155.1 jit_solution(13238885284118356484)
XLA Ops:
  0.6 0.0 copy-start
  0.6 0.0 copy-start.2
  0.7 0.0 copy-start.4
  0.7 1.0 constant_dynamic-slice_fusion.1
  1.6 1.5 pad_maximum_fusion.kv_ref
  3.2 0.8 select_reduce_fusion.4
  4.0 0.7 select_reduce_fusion.1
  4.7 0.6 pad_maximum_fusion.1.side_ref
  5.3 1.5 fusion
  6.8 0.0 copy-done.2
  6.8 0.0 copy-done.4
  6.8 0.3 fusion.2.x_ref
  7.1 0.0 copy-done
  7.1 0.0 copy-start.1
  7.2 0.0 copy-start.6
  7.2 0.4 fusion.22
  7.6 1.0 copy-done.6
  8.6 1.0 fusion.5.sact_ref
  9.6 0.0 copy-done.1
  9.6 0.0 copy-start.7
  9.6 120.4 %shard_map.176 = (bf16[256,2048]{1,0:T(8,128)(2,1)}, bf16[8,128,512]{2,1,0:T(8,128)(2,1)}, f32[8,16,256]{2,1,0:T(8,128)}, bf16[4,256,512]{2,1,0:T(8,128)(2,1)}) custom-call(bf16[256,2048]{1,0:T(8,128)(2,1)} %copy-done.1, f32[16,256]{1,0:T(8,128)} %pad_maximum_fusion.1.side_ref, bf16[128,512]{1,0:T(8,128)(2,1)} %pad_maximum_fusion.kv_ref, ...), custom_call_target="tpu_custom_call" | custom-call | tf_op jit(solution)/shard_map/pallas_call | solution.py:521
  130.0 0.8 slice_bitcast_fusion
  130.8 0.3 reduce_window_sum.13
  131.1 0.2 slice_reduce_fusion
  131.2 0.1 select_reduce_fusion.2
  131.4 0.1 broadcast_select_fusion
  131.5 1.9 %select_reduce_fusion = f32[128]{0:T(128)S(1)} fusion(f32[8,128]{1,0:T(8,128)S(1)} %bitcast.56, f32[128]{0:T(128)S(1)} %fusion.20, pred[8]{0:T(512)(128)(4,1)S(1)} %get-tuple-element.15, pred[128,128]{1,0:T(8,128)(4,1)S(1)} %iota_compare_fusion, pred[8]{0:T(512)(128)(4,1)S(1)} %get-tuple-element.14), kind=kLoop, calls=%fused_computation.14 | loop fusion | flops 655232 | bytes 21520 | tf_op jit(solution)/shard_map/reduce_max | solution.py:70
  133.3 0.6 fusion.14
  134.0 0.7 bitcast_maximum_fusion
  134.6 0.1 broadcast_bitcast_fusion
  134.7 0.1 broadcast_bitcast_fusion.1
  134.8 0.1 and.56
  134.8 0.0 copy-done.7
  134.8 0.0 copy-start.5
  134.9 0.0 copy-start.8
  134.9 1.6 %fusion.21 = (f32[128]{0:T(128)S(1)}, bf16[128,1024]{1,0:T(8,128)(2,1)S(1)}) fusion(f32[128]{0:T(128)S(1)} %bitcast_maximum_fusion, f32[1024]{0:T(1024)S(1)} %bitcast.57, f32[128]{0:T(128)S(1)} %fusion.20, pred[16,8,8,128]{3,2,1,0:T(8,128)(4,1)S(1)} %bitcast.53, pred[1024]{0:T(1024)(128)(4,1)S(1)} %broadcast_bitcast_fusion, ...), kind=kOutput, calls=%fused_computation.57 | convolution fusion | flops 68288384 | bytes 990724 | tf_op jit(solution)/shard_map/td,sd->ts/dot_general | solution.py:73
  136.5 0.0 copy-done.5
  136.5 0.0 copy-done.8
  136.5 0.9 fusion.6.gated_ref
  137.4 0.0 copy-start.3
  137.4 14.9 %shard_map.177 = bf16[128,2048]{1,0:T(8,128)(2,1)} custom-call(bf16[128,256]{1,0:T(8,128)(2,1)} %fusion.6.gated_ref, bf16[4,256,512]{2,1,0:T(8,128)(2,1)} %get-tuple-element.8.mwq_ref), custom_call_target="tpu_custom_call" | custom-call | tf_op jit(solution)/shard_map/pallas_call | solution.py:568
  152.3 1.9 %copy.27 = bf16[128,2048]{1,0:T(8,128)(2,1)} copy(bf16[128,2048]{1,0:T(8,128)(2,1)} %shard_map.177) | data formatting | bytes 1048576
  154.1 0.0 copy-done.3
  154.2 1.0 copy.28
  (9 shorter events, 0.1 us)
Async XLA Ops:
  0.6 6.5 %copy-start = (bf16[2048,128]{1,0:T(8,128)(2,1)S(1)}, bf16[2048,128]{1,0:T(8,128)(2,1)}, u32[]{:S(2)}) copy-start(bf16[2048,128]{1,0:T(8,128)(2,1)} %param.31) | copy-start | bytes 1572868
  0.6 6.2 %copy-start.2 = (bf16[256,2048]{1,0:T(8,128)(2,1)S(1)}, bf16[256,2048]{1,0:T(8,128)(2,1)}, u32[]{:S(2)}) copy-start(bf16[256,2048]{1,0:T(8,128)(2,1)} %param.24) | copy-start | bytes 3145732
  0.7 6.2 %copy-start.4 = (f32[2048]{0:T(1024)S(1)}, f32[2048]{0:T(1024)}, u32[]{:S(2)}) copy-start(f32[2048]{0:T(1024)} %param.25) | copy-start | bytes 24580
  7.1 2.5 %copy-start.1 = (bf16[256,2048]{1,0:T(8,128)(2,1)}, bf16[256,2048]{1,0:T(8,128)(2,1)S(1)}, u32[]{:S(2)}) copy-start(bf16[256,2048]{1,0:T(8,128)(2,1)S(1)} %fusion.2.x_ref) | copy-start | bytes 3145732
  7.2 1.4 copy-start.6
  9.6 125.2 %copy-start.7 = (bf16[128,512]{1,0:T(8,128)(2,1)S(1)}, bf16[128,512]{1,0:T(8,128)(2,1)}, u32[]{:S(2)}) copy-start(bf16[128,512]{1,0:T(8,128)(2,1)} %param.17) | copy-start | bytes 393220
  134.8 1.6 %copy-start.5 = (bf16[8,128,512]{2,1,0:T(8,128)(2,1)S(1)}, bf16[8,128,512]{2,1,0:T(8,128)(2,1)}, u32[]{:S(2)}) copy-start(bf16[8,128,512]{2,1,0:T(8,128)(2,1)} %get-tuple-element.6) | copy-start | bytes 3145732
  134.9 1.6 %copy-start.8 = (bf16[128,256]{1,0:T(8,128)(2,1)S(1)}, bf16[128,256]{1,0:T(8,128)(2,1)}, u32[]{:S(2)}) copy-start(bf16[128,256]{1,0:T(8,128)(2,1)} %param.20) | copy-start | bytes 196612
  137.4 16.8 %copy-start.3 = (bf16[256,2048]{1,0:T(8,128)(2,1)S(1)}, bf16[256,2048]{1,0:T(8,128)(2,1)}, u32[]{:S(2)}) copy-start(bf16[256,2048]{1,0:T(8,128)(2,1)} %get-tuple-element.21) | copy-start | bytes 3145732
